TPU v7x, 128 devices: a whole 4x4x4 slice. The times are simulated.
128 devices in a mesh: fs: 32 (over z, y, core), tp: 4 (over x).
Axes of the slice: x: 4, y: 4, z: 4, core: 2. Of those that a mesh axis runs over, the one named last changes fastest.
Arguments:
- model_input: bfloat16 [65536, 2048], P('fs'), may hold values from -6 to 6
- value_cotan: bfloat16 [65536, 2048], P('fs', 'tp'), may hold values from -0.0234375 to 0.0234375
- mixer_cotan: bfloat16 [65536, 2048], P('fs'), may hold values from -0.0234375 to 0.0234375
- head_output: bfloat16 [65536, 2048], P('fs', 'tp'), may hold values from -6 to 6
- value_weight: float32 [2048, 2048], P('fs', 'tp'), may hold values from -0.125 to 0.125
- value_factor: bfloat16 [2048, 512], P('fs'), may hold values from -0.125 to 0.125
- value_first: float32 [512, 2048], P('fs', 'tp'), may hold values from -3 to 3
- value_second: float32 [512, 2048], P('fs', 'tp'), may hold values from 0.02 to 0.5
- output_weight: float32 [2048, 2048], P('fs', 'tp'), may hold values from -0.125 to 0.125
- output_factor: bfloat16 [2048, 512], P('fs'), may hold values from -0.125 to 0.125
- output_first: float32 [512, 2048], P('fs', 'tp'), may hold values from -3 to 3
- output_second: float32 [512, 2048], P('fs', 'tp'), may hold values from 0.02 to 0.5
Outputs:
- value_step: float32 [2048, 2048], P('fs', 'tp')
- value_updated: float32 [2048, 2048], P('fs', 'tp')
- value_first_new: float32 [512, 2048], P('fs', 'tp')
- value_second_new: float32 [512, 2048], P('fs', 'tp')
- value_copy: bfloat16 [2048, 2048], P(None, 'tp')
- output_step: float32 [2048, 2048], P('fs', 'tp')
- output_updated: float32 [2048, 2048], P('fs', 'tp')
- output_first_new: float32 [512, 2048], P('fs', 'tp')
- output_second_new: float32 [512, 2048], P('fs', 'tp')
- output_copy: bfloat16 [2048, 2048], P(None, 'tp')
All inputs are finite; a program needn't handle non-finite values.
Results may differ from a plain program's by a relative error of at most 0.0059.
Values may be sent and summed in bfloat16 or wider, within the bound.
A program may use at most 128 MiB of HBM per device.

v0:
```python
import functools

import jax
import jax.numpy as jnp
from jax import lax
from jax.experimental import pallas as pl
from jax.experimental.pallas import tpu as pltpu
from jax.sharding import PartitionSpec as P

beta_first = 0.8
beta_second = 0.9
step_rate = 0.02
scale_floor = 0.25
tiny_eps = 1e-08

MESH = pl.DeviceIdType.MESH
F32 = jnp.float32
BF16 = jnp.bfloat16
VMEM_LIMIT = 67_000_000
W_HOOK = (0, 1, 2)


def kernel(
    n,
    ntp,
    rows_v, cols_v, rows_o, cols_o,
    fac_ref, w_v, w_o, first_v, first_o, second_v, second_o,
    step_v, upd_v, fnew_v, snew_v, copy_v,
    step_o, upd_o, fnew_o, snew_o, copy_o,
    rows, cols, fg, wg, acc, e_buf, pf, pg, send_a, recv_a, send_b, recv_b,
    dirg, ss, ssg,
    sem_rows, sem_cols,
    fs_z, fr_z, fs_y, fr_y, fs_c, fr_c,
    ws_z, wr_z, ws_y, wr_y,
    as_, ar, bs, br,
    ds_z, dr_z, ds_y, dr_y,
    ps, pr,
):
    nz = n // 2
    me = lax.axis_index("fs")
    tp = lax.axis_index("tp")
    z, y = me // 2, lax.rem(me, 2)
    ybar = 1 - y
    mate = 2 * z + ybar
    core = lax.rem(tp, 2)
    other = 1 - core
    twin = tp + 1 - 2 * core
    T, D = rows_v.shape
    C = cols_v.shape[1]
    R, K = fac_ref.shape[1:]
    k = first_v.shape[0]
    TC = 512

    def zup(d):
        return lax.rem(z + d, nz)

    def zdn(d):
        return lax.rem(z + nz - d, nz)

    def rcopy(src, dst, ssem, rsem, dev):
        return pltpu.make_async_remote_copy(
            src_ref=src, dst_ref=dst, send_sem=ssem, recv_sem=rsem,
            device_id=dev, device_id_type=MESH,
        )

    def fsdev(i):
        return (i, tp)

    loads = []
    for m, (r, c) in enumerate(((rows_v, cols_v), (rows_o, cols_o))):
        loads.append(pltpu.make_async_copy(r, rows.at[m], sem_rows.at[m]))
        loads.append(pltpu.make_async_copy(c, cols.at[m], sem_cols.at[m]))
    for i in (0, 2, 1, 3):
        loads[i].start()

    barrier = pltpu.get_barrier_semaphore()
    for d in range(1, nz):
        pl.semaphore_signal(
            barrier, inc=1, device_id=fsdev(2 * zup(d) + y), device_id_type=MESH
        )
    pl.semaphore_signal(barrier, inc=1, device_id=fsdev(mate), device_id_type=MESH)
    for q in range(1, ntp):
        pl.semaphore_signal(
            barrier, inc=1, device_id=(me, lax.rem(tp + q, ntp)), device_id_type=MESH
        )
    pl.semaphore_wait(barrier, nz - 1 + 1 + ntp - 1)

    pend = []

    for d in list(range(1, nz)):
        c = rcopy(fac_ref.at[core], fg.at[core, me], fs_z.at[d], fr_z.at[d], fsdev(2 * zup(d) + y))
        c.start()
        pend.append(c)
    c = rcopy(fac_ref.at[core], fg.at[core, me], fs_y.at[0], fr_y.at[0], fsdev(mate))
    c.start()
    pend.append(c)
    for m in range(2):
        fg[m, me] = fac_ref[m]
    wg[me, 0] = w_v[...].astype(BF16)
    wg[me, 1] = w_o[...].astype(BF16)

    def w_send(d):
        if d == 0:
            c = rcopy(wg.at[me], wg.at[me], ws_y.at[0], wr_y.at[0], fsdev(mate))
        else:
            c = rcopy(wg.at[me], wg.at[me], ws_z.at[d], wr_z.at[d], fsdev(2 * zup(d) + y))
        c.start()
        pend.append(c)

    def w_forward(d):
        i = 2 * zdn(d) + y
        rcopy(wg.at[i], wg.at[i], ws_z.at[d], wr_z.at[d], fsdev(mate)).wait_recv()
        c = rcopy(wg.at[i], wg.at[i], ws_y.at[d], wr_y.at[d], fsdev(mate))
        c.start()
        pend.append(c)

    def w_finish(d):
        i = 2 * zdn(d) + ybar
        rcopy(wg.at[i], wg.at[i], ws_y.at[d], wr_y.at[d], fsdev(mate)).wait_recv()

    def to_twin(i, q):
        c = rcopy(fg.at[core, i], fg.at[core, i], fs_c.at[q], fr_c.at[q], (me, twin))
        c.start()
        pend.append(c)

    def f_recv(sems, d, i):
        rcopy(fg.at[core, i], fg.at[core, i], fs_z.at[0], sems.at[d], fsdev(mate)).wait_recv()

    def f_recv_twin(i, q):
        rcopy(fg.at[other, i], fg.at[other, i], fs_c.at[0], fr_c.at[q], (me, twin)).wait_recv()

    def accumulate(m, d):
        p = zdn(d)
        pair = jnp.concatenate([fg[m, 2 * p], fg[m, 2 * p + 1]], axis=0)
        pair_t = pair.T

        @pl.loop(0, T // TC)
        def _(t):
            at = pl.ds(pl.multiple_of(t * TC, TC), TC)
            lhs = rows[m, at, pl.ds(pl.multiple_of(p * 2 * R, 2 * R), 2 * R)]
            prod = lax.dot_general(
                pair_t, lhs, (((1,), (1,)), ((), ())), preferred_element_type=F32
            )
            if d == 0:
                acc[m, :, at] = prod
            else:
                acc[m, :, at] += prod

    for d in range(nz):
        if d > 0:
            i = 2 * zdn(d) + y
            f_recv(fr_z, d, i)
            c = rcopy(fg.at[core, i], fg.at[core, i], fs_y.at[d], fr_y.at[d], fsdev(mate))
            c.start()
            pend.append(c)
            to_twin(i, 2 * d)
        i = 2 * zdn(d) + ybar
        f_recv(fr_y, d, i)
        to_twin(i, 2 * d + 1)
        if d == 0:
            for h in range(nz):
                if h < len(W_HOOK) and W_HOOK[h] == 0 or h >= len(W_HOOK):
                    w_send(h)
            loads[0].wait()
            loads[2].wait()
        accumulate(core, d)
        if d > 0:
            f_recv_twin(2 * zdn(d) + y, 2 * d)
        f_recv_twin(i, 2 * d + 1)
        accumulate(other, d)
    loads[1].wait()
    loads[3].wait()

    def hook(v):
        for h in range(min(nz, len(W_HOOK))):
            if W_HOOK[h] == v:
                w_send(h)

    def partial_products(m):
        @pl.loop(0, T // TC)
        def _(t):
            at = pl.ds(pl.multiple_of(t * TC, TC), TC)
            red = acc[m, :, at].astype(BF16)
            prod = jnp.dot(red, cols[m, at, :], preferred_element_type=F32)
            prod = prod.reshape(n, k, C)

            @pl.when(t == 0)
            def _():
                pf[m] = prod

            @pl.when(t > 0)
            def _():
                pf[m] += prod

        for h in range(nz):
            send_a[m, h] = pf[m, 2 * zup(h) + ybar].astype(BF16)
        for h in [*range(1, nz), 0]:
            c = rcopy(
                send_a.at[m, h], recv_a.at[m, h], as_.at[m, h], ar.at[m, h], fsdev(mate)
            )
            c.start()
            pend.append(c)

    def middle(m):
        for h in [*range(1, nz), 0]:
            rcopy(
                send_a.at[m, h], recv_a.at[m, h], as_.at[m, h], ar.at[m, h], fsdev(mate)
            ).wait_recv()
            tot = pf[m, 2 * zup(h) + y] + recv_a[m, h].astype(F32)
            if h == 0:
                pg[m] = tot
            else:
                send_b[m, h] = tot.astype(BF16)
                c = rcopy(
                    send_b.at[m, h], recv_b.at[m, h], bs.at[m, h], br.at[m, h],
                    fsdev(2 * zup(h) + y),
                )
                c.start()
                pend.append(c)

    def moments(m, first, second, fnew, snew):
        tot = pg[m]
        for h in range(1, nz):
            rcopy(
                send_b.at[m, h], recv_b.at[m, h], bs.at[m, h], br.at[m, h], fsdev(mate)
            ).wait_recv()
            tot = tot + recv_b[m, h].astype(F32)
        f = beta_first * first[...] + (1.0 - beta_first) * tot
        s = beta_second * second[...] + (1.0 - beta_second) * tot * tot
        fnew[...] = f
        snew[...] = s
        dirg[m, me] = (f / (jnp.sqrt(s) + tiny_eps)).astype(BF16)
        for h in range(1, nz):
            c = rcopy(
                dirg.at[m, me], dirg.at[m, me], ds_z.at[m, h], dr_z.at[m, h],
                fsdev(2 * zup(h) + y),
            )
            c.start()
            pend.append(c)
        c = rcopy(dirg.at[m, me], dirg.at[m, me], ds_y.at[m, 0], dr_y.at[m, 0], fsdev(mate))
        c.start()
        pend.append(c)

    def dir_forward(m):
        for h in range(1, nz):
            i = 2 * zdn(h) + y
            rcopy(
                dirg.at[m, i], dirg.at[m, i], ds_z.at[m, h], dr_z.at[m, h], fsdev(mate)
            ).wait_recv()
            c = rcopy(dirg.at[m, i], dirg.at[m, i], ds_y.at[m, h], dr_y.at[m, h], fsdev(mate))
            c.start()
            pend.append(c)

    def expand(m):
        for h in range(nz):
            i = 2 * zdn(h) + ybar
            rcopy(
                dirg.at[m, i], dirg.at[m, i], ds_y.at[m, h], dr_y.at[m, h], fsdev(mate)
            ).wait_recv()
        ss[m] = jnp.zeros(ss.shape[1:], F32)

        @pl.loop(0, nz)
        def _(b):
            lhs = fg[m, pl.ds(2 * b, 2)].reshape(2 * R, K)
            ex = jnp.dot(lhs, dirg[m].reshape(n * k, C), preferred_element_type=F32)
            e_buf[m, pl.ds(2 * b, 2)] = ex.reshape(2, R, C)
            ss[m] += jnp.sum((ex * ex).reshape(2 * R // 8, 8, C), axis=0)

        for q in range(1, ntp):
            c = rcopy(
                ss.at[m], ssg.at[m, q], ps.at[m, q], pr.at[m, q],
                (me, lax.rem(tp + q, ntp)),
            )
            c.start()
            pend.append(c)

    def finish(m, weight, step, upd, copy):
        tot = ss[m]
        for q in range(1, ntp):
            rcopy(ss.at[m], ssg.at[m, q], ps.at[m, q], pr.at[m, q], (me, twin)).wait_recv()
            tot = tot + ssg[m, q]
        mean = jnp.sum(tot, keepdims=True) / (n * R * C * ntp)
        scale = step_rate / jnp.sqrt(mean + scale_floor)
        s = scale * e_buf[m, me]
        step[...] = s
        upd[...] = weight[...] - s

        @pl.loop(0, n)
        def _(b):
            at = pl.ds(pl.multiple_of(b * R, R), R)
            copy[at, :] = (wg[b, m].astype(F32) - scale * e_buf[m, b]).astype(BF16)

    partial_products(0)
    partial_products(1)
    middle(0)
    middle(1)
    hook(1)
    moments(0, first_v, second_v, fnew_v, snew_v)
    moments(1, first_o, second_o, fnew_o, snew_o)
    hook(2)
    dir_forward(0)
    dir_forward(1)
    expand(0)
    expand(1)
    for h in range(1, nz):
        w_forward(h)
    for h in range(nz):
        w_finish(h)
    finish(0, w_v, step_v, upd_v, copy_v)
    finish(1, w_o, step_o, upd_o, copy_o)
    for c in pend:
        c.wait_send()


def local(
    n, ntp,
    model_input, value_cotan, mixer_cotan, head_output,
    value_weight, value_factor, value_first, value_second,
    output_weight, output_factor, output_first, output_second,
):
    T, D = model_input.shape
    C = value_cotan.shape[1]
    R, K = value_factor.shape
    k = value_first.shape[0]
    nz = n // 2
    vm = pl.BlockSpec(memory_space=pltpu.VMEM)
    hbm = pl.BlockSpec(memory_space=pl.ANY)
    wide = jax.ShapeDtypeStruct((R, C), F32)
    mom = jax.ShapeDtypeStruct((k, C), F32)
    full = jax.ShapeDtypeStruct((n * R, C), BF16)
    dma = pltpu.SemaphoreType.DMA
    return pl.pallas_call(
        functools.partial(kernel, n, ntp),
        out_shape=(wide, wide, mom, mom, full) * 2,
        in_specs=[hbm] * 4 + [vm] * 7,
        out_specs=(vm,) * 10,
        scratch_shapes=[
            pltpu.VMEM((2, T, D), BF16),
            pltpu.VMEM((2, T, C), BF16),
            pltpu.VMEM((2, n, R, K), BF16),
            pltpu.VMEM((n, 2, R, C), BF16),
            pltpu.VMEM((2, K, T), F32),
            pltpu.VMEM((2, n, R, C), F32),
            pltpu.VMEM((2, n, k, C), F32),
            pltpu.VMEM((2, k, C), F32),
            pltpu.VMEM((2, nz, k, C), BF16),
            pltpu.VMEM((2, nz, k, C), BF16),
            pltpu.VMEM((2, nz, k, C), BF16),
            pltpu.VMEM((2, nz, k, C), BF16),
            pltpu.VMEM((2, n, k, C), BF16),
            pltpu.VMEM((2, 8, C), F32),
            pltpu.VMEM((2, ntp, 8, C), F32),
            dma((2,)), dma((2,)),
            dma((nz,)), dma((nz,)), dma((nz,)), dma((nz,)), dma((n,)), dma((n,)),
            dma((nz,)), dma((nz,)), dma((nz,)), dma((nz,)),
            dma((2, nz)), dma((2, nz)), dma((2, nz)), dma((2, nz)),
            dma((2, nz)), dma((2, nz)), dma((2, nz)), dma((2, nz)),
            dma((2, ntp)), dma((2, ntp)),
        ],
        compiler_params=pltpu.CompilerParams(
            collective_id=0, has_side_effects=True, vmem_limit_bytes=VMEM_LIMIT
        ),
    )(
        model_input, value_cotan, mixer_cotan, head_output,
        jnp.stack([value_factor, output_factor]),
        value_weight, output_weight,
        value_first, output_first, value_second, output_second,
    )


def solution(mesh):
    rows, both, full = P("fs", None), P("fs", "tp"), P(None, "tp")
    return jax.shard_map(
        functools.partial(local, mesh.shape["fs"], mesh.shape["tp"]),
        mesh=mesh,
        in_specs=(rows, both, rows, both) + (both, rows, both, both) * 2,
        out_specs=(both, both, both, both, full) * 2,
        check_vma=False,
    )
```

profile of v0, /device:TPU:1, one launch (start us, length us, event | category | flops | bytes accessed | tf_op | source)
XLA Modules:
  0.0 165.9 jit_solution(6442147559480576829)
XLA Ops:
  0.6 1.5 pad_maximum_fusion.fac_ref
  2.2 150.8 %shard_map.195 = (f32[64,512]{1,0:T(8,128)}, f32[64,512]{1,0:T(8,128)}, f32[16,512]{1,0:T(8,128)}, f32[16,512]{1,0:T(8,128)}, bf16[2048,512]{1,0:T(8,128)(2,1)},...) custom-call(bf16[2048,2048]{1,0:T(8,128)(2,1)} %rows_v.1, ...), custom_call_target="tpu_custom_call" | custom-call | tf_op jit(solution)/shard_map/pallas_call | solution.py:332
  152.9 1.6 copy.32
  154.5 1.6 copy.33
  156.1 1.4 copy.34
  157.5 1.4 copy.35
  158.8 0.0 copy-start.2
  158.8 0.0 copy-start.1
  158.8 0.0 copy-start.4
  158.8 0.0 copy-start.3
  158.8 0.0 copy-start
  158.9 3.2 %copy.36 = bf16[2048,512]{1,0:T(8,128)(2,1)} copy(bf16[2048,512]{1,0:T(8,128)(2,1)} %get-tuple-element.24) | data formatting | bytes 4194304
  162.0 0.0 copy-done.2
  162.1 0.7 copy.37
  162.7 0.0 copy-done.1
  162.7 0.7 copy.38
  163.4 0.0 copy-done.4
  163.4 0.6 copy.39
  164.0 0.0 copy-done.3
  164.0 0.6 copy.40
  164.6 0.0 copy-done
  164.6 1.3 copy.41
Async XLA Ops:
  158.8 3.2 %copy-start.2 = (f32[64,512]{1,0:T(8,128)S(1)}, f32[64,512]{1,0:T(8,128)}, u32[]{:S(2)}) copy-start(f32[64,512]{1,0:T(8,128)} %get-tuple-element.25) | copy-start | bytes 393220
  158.8 3.9 %copy-start.1 = (f32[64,512]{1,0:T(8,128)S(1)}, f32[64,512]{1,0:T(8,128)}, u32[]{:S(2)}) copy-start(f32[64,512]{1,0:T(8,128)} %get-tuple-element.26) | copy-start | bytes 393220
  158.8 4.5 %copy-start.4 = (f32[16,512]{1,0:T(8,128)S(1)}, f32[16,512]{1,0:T(8,128)}, u32[]{:S(2)}) copy-start(f32[16,512]{1,0:T(8,128)} %get-tuple-element.27) | copy-start | bytes 98308
  158.8 5.1 %copy-start.3 = (f32[16,512]{1,0:T(8,128)S(1)}, f32[16,512]{1,0:T(8,128)}, u32[]{:S(2)}) copy-start(f32[16,512]{1,0:T(8,128)} %get-tuple-element.28) | copy-start | bytes 98308
  158.8 5.8 %copy-start = (bf16[2048,512]{1,0:T(8,128)(2,1)S(1)}, bf16[2048,512]{1,0:T(8,128)(2,1)}, u32[]{:S(2)}) copy-start(bf16[2048,512]{1,0:T(8,128)(2,1)} %get-tuple-element.29) | copy-start | bytes 6291460
where the time goes:
time: 166 us
  Pallas kernels  151 us (91%)
  local copies, waits for them, and re-layouts  13 us (8%)
    pallas_call x1, Pallas kernels, local(): pl.pallas_call(functools.partial(kernel, n, ntp), out_shape=(wide, wide,...  151 us
    unnamed x20, local copies, waits for them, and re-layouts  13 us

commit v1 on v0

v1 whole, which is shorter than its diff:
```python
import functools

import jax
import jax.numpy as jnp
from jax import lax
from jax.experimental import pallas as pl
from jax.experimental.pallas import tpu as pltpu
from jax.sharding import PartitionSpec as P

beta_first = 0.8
beta_second = 0.9
step_rate = 0.02
scale_floor = 0.25
tiny_eps = 1e-08

MESH = pl.DeviceIdType.MESH
F32 = jnp.float32
BF16 = jnp.bfloat16
NZ = 4
NC = 2
NQ = 4
WS = 4
GN = 256
N_SEMS = 240
OFFSETS = sorted(
    [(a, b) for a in range(NZ) for b in range(NZ) if a or b],
    key=lambda o: -(min(o[0], NZ - o[0]) + min(o[1], NZ - o[1])),
)


def gather_kernel(
    ntp,
    rows_v, cols_v, rows_o, cols_o,
    fac_v, fac_o, w_v, w_o, first_v, first_o, second_v, second_o,
    fnew_v, snew_v, fnew_o, snew_o, ss_out, fg_out, wg_out, dir_out,
    rows, cols, cols_t, grad, fg, wg, pf, send_a, recv_a, send_b, recv_b, pg,
    dirg, gram, ss, ssg,
    sem_rows, sem_cols, sem_out, ssem, rsem,
):
    me = lax.axis_index("fs")
    tp = lax.axis_index("tp")
    z, y, c = me // (NZ * NC), lax.rem(me // NC, NZ), lax.rem(me, NC)
    co = 1 - c
    chip = z * NZ + y
    h = lax.rem(tp, 2)
    T, D = rows_v.shape
    C = cols_v.shape[1]
    R = fac_v.shape[1]
    QR = fac_v.shape[0] // NQ
    WR = w_v.shape[0] // WS

    def up(a, d):
        return lax.rem(a + d, NZ)

    def dn(a, d):
        return lax.rem(a + NZ - d, NZ)

    def plane(zz, yy):
        return ((zz * NZ + yy) * NC + c, tp)

    mate = (me - c + co, tp)

    def along_x(d):
        return (me, lax.rem(tp + ntp + d, ntp))

    n_used = [0]
    pend = []

    class Send:
        def __init__(self, src, dst, landed, dev):
            i = n_used[0]
            n_used[0] += 1
            self.copy = pltpu.make_async_remote_copy(
                src_ref=src, dst_ref=dst, send_sem=ssem.at[i], recv_sem=rsem.at[i],
                device_id=dev, device_id_type=MESH,
            )
            self.twin = pltpu.make_async_remote_copy(
                src_ref=landed, dst_ref=landed, send_sem=ssem.at[i], recv_sem=rsem.at[i],
                device_id=dev, device_id_type=MESH,
            )

        def start(self):
            self.copy.start()
            pend.append(self.copy)

        def arrived(self):
            self.twin.wait_recv()

    row_loads, col_loads = [[], []], []
    half = D // 4
    for m, (r, cc) in enumerate(((rows_v, cols_v), (rows_o, cols_o))):
        cl = pltpu.make_async_copy(cc, cols.at[m], sem_cols.at[m])
        cl.start()
        col_loads.append(cl)
        for j in range(4):
            at = pl.ds(j * half, half)
            rl = pltpu.make_async_copy(r.at[:, at], rows.at[m, :, at], sem_rows.at[m, j])
            rl.start()
            row_loads[m].append(rl)

    barrier = pltpu.get_barrier_semaphore()
    for dz, dy in OFFSETS:
        pl.semaphore_signal(barrier, inc=1, device_id=plane(up(z, dz), up(y, dy)), device_id_type=MESH)
    pl.semaphore_signal(barrier, inc=1, device_id=mate, device_id_type=MESH)
    for q in range(1, ntp):
        pl.semaphore_signal(barrier, inc=1, device_id=along_x(q), device_id_type=MESH)

    for m, f in enumerate((fac_v, fac_o)):
        for s in range(2):
            k = 2 * h + s
            fg[m, z, y, c, k] = f[pl.ds(pl.multiple_of(k * QR, QR), QR), :]
    for m, w in enumerate((w_v, w_o)):
        for j in range(WS):
            wg[m, z, y, c, j] = w[pl.ds(j * WR, WR), :].astype(BF16)

    def line(buf, m, s, g, cc, k):
        return buf.at[m, :, dn(y, g), cc, k] if s == 0 else buf.at[m, dn(z, g), :, cc, k]

    def own(buf, m, s, d, k):
        return buf.at[m, dn(z, d), y, c, k] if s == 0 else buf.at[m, z, dn(y, d), c, k]

    def first_dev(s, d):
        return plane(up(z, d), y) if s == 0 else plane(z, up(y, d))

    def second_dev(s, d):
        return plane(z, up(y, d)) if s == 0 else plane(up(z, d), y)

    f1, f2, fx, fm, fxm = {}, {}, {}, {}, {}
    for m in range(2):
        for s in range(2):
            k, kx = 2 * h + s, 2 * (1 - h) + s
            for d in (2, 1, 3):
                f1[m, s, d] = Send(own(fg, m, s, 0, k), own(fg, m, s, 0, k), own(fg, m, s, d, k), first_dev(s, d))
                f2[m, s, d] = Send(line(fg, m, s, 0, c, k), line(fg, m, s, 0, c, k), line(fg, m, s, d, c, k), second_dev(s, d))
            for g in range(NZ):
                a, b = line(fg, m, s, g, c, k), line(fg, m, s, g, c, kx)
                fx[m, s, g] = Send(a, a, b, along_x(1 if s == 0 else -1))
                fm[m, s, g] = Send(a, a, line(fg, m, s, g, co, k), mate)
                fxm[m, s, g] = Send(b, b, line(fg, m, s, g, co, kx), mate)

    def f_first(m):
        for d in (2, 1, 3):
            for s in range(2):
                f1[m, s, d].start()

    def f_second(m):
        for s in range(2):
            for d in (1, 3, 2):
                f1[m, s, d].arrived()
            for d in (2, 1, 3):
                f2[m, s, d].start()
            fx[m, s, 0].start()
            fm[m, s, 0].start()

    def f_across(m, gs):
        for g in gs:
            for s in range(2):
                f2[m, s, g].arrived()
                fx[m, s, g].start()
                fm[m, s, g].start()

    def f_mate(m, gs):
        for g in gs:
            for s in range(2):
                fx[m, s, g].arrived()
                fxm[m, s, g].start()

    f_outs = []

    def f_done(m):
        for g in (0, 1, 3, 2):
            for s in range(2):
                fm[m, s, g].arrived()
                fxm[m, s, g].arrived()
        o = pltpu.make_async_copy(fg.at[m], fg_out.at[m], sem_out.at[m])
        o.start()
        f_outs.append(o)

    w1, w2, wm = {}, {}, {}
    for m in range(2):
        for j in range(WS):
            for d in (2, 1, 3):
                w1[m, j, d] = Send(own(wg, m, m, 0, j), own(wg, m, m, 0, j), own(wg, m, m, d, j), first_dev(m, d))
                w2[m, j, d] = Send(line(wg, m, m, 0, c, j), line(wg, m, m, 0, c, j), line(wg, m, m, d, c, j), second_dev(m, d))
        for g in range(NZ):
            def whole(cc, m=m, g=g):
                return wg.at[m, :, dn(y, g), cc] if m == 0 else wg.at[m, dn(z, g), :, cc]

            wm[m, g] = Send(whole(c), whole(c), whole(co), mate)

    def w_first():
        for j in range(WS):
            for d in (2, 1, 3):
                for m in range(2):
                    w1[m, j, d].start()

    def w_second(js):
        for j in js:
            for m in range(2):
                for d in (1, 3, 2):
                    w1[m, j, d].arrived()
            for d in (2, 1, 3):
                for m in range(2):
                    w2[m, j, d].start()

    def w_mate(gs):
        for g in gs:
            for m in range(2):
                if g:
                    for j in range(WS):
                        w2[m, j, g].arrived()
                wm[m, g].start()

    def turn_cols(m):
        col_loads[m].wait()
        for t in range(4):
            at = pl.ds(t * (T // 4), T // 4)
            cols_t[m, :, at] = cols[m, at, :].T

    def gradient(m, n):
        if n % (half // GN) == 0:
            row_loads[m][n // (half // GN)].wait()
        at = pl.ds(n * GN, GN)
        grad[m, :, at] = jnp.dot(cols_t[m], rows[m, :, at], preferred_element_type=F32).astype(BF16)

    def factor_of(m):
        return fg[m].reshape(D, R)

    sa, sb = {}, {}
    for m in range(2):
        sa[m] = Send(send_a.at[m], recv_a.at[m], recv_a.at[m], mate)
        for i, (dz, dy) in enumerate(OFFSETS):
            to = up(z, dz) * NZ + up(y, dy)
            sb[m, i] = Send(send_b.at[m, to], recv_b.at[m, i], recv_b.at[m, i], plane(up(z, dz), up(y, dy)))

    def project(m):
        f = factor_of(m)
        for b in range(2):
            w = R // 2
            pt = jnp.dot(grad[m], f[:, b * w:(b + 1) * w], preferred_element_type=F32)
            pf[m, pl.ds(b * NZ * NZ // 2, NZ * NZ // 2)] = pt.T.reshape(NZ * NZ // 2, NC, QR, C)
        send_a[m] = pf[m, :, co].astype(BF16)
        sa[m].start()

    def scatter(m):
        sa[m].arrived()
        send_b[m] = (pf[m, :, c] + recv_a[m].astype(F32)).astype(BF16)
        for i in range(len(OFFSETS)):
            sb[m, i].start()
        pg[m] = pf[m, chip, c] + recv_a[m, chip].astype(F32)

    dp, dm, dmo = {}, {}, {}
    for m in range(2):
        mine = dirg.at[m, chip, c]
        dmo[m] = Send(mine, mine, dirg.at[m, chip, co], mate)
        for i, (dz, dy) in enumerate(OFFSETS):
            frm = dn(z, dz) * NZ + dn(y, dy)
            dp[m, i] = Send(mine, mine, dirg.at[m, frm, c], plane(up(z, dz), up(y, dy)))
            dm[m, i] = Send(dirg.at[m, frm, c], dirg.at[m, frm, c], dirg.at[m, frm, co], mate)

    def moments(m, first, second, fnew, snew):
        tot = pg[m]
        for i in range(len(OFFSETS)):
            sb[m, i].arrived()
            tot = tot + recv_b[m, i].astype(F32)
        f = beta_first * first[...] + (1.0 - beta_first) * tot
        s = beta_second * second[...] + (1.0 - beta_second) * tot * tot
        dirg[m, chip, c] = (f / (jnp.sqrt(s) + tiny_eps)).astype(BF16)
        for i in range(len(OFFSETS)):
            dp[m, i].start()
        dmo[m].start()
        fnew[...] = f
        snew[...] = s

    def spread(m):
        for i in range(len(OFFSETS)):
            dp[m, i].arrived()
            dm[m, i].start()

    def gram_of(m):
        f = factor_of(m)
        ft = f.T
        g = jnp.dot(ft, f, preferred_element_type=F32)
        hi = g.astype(BF16)
        gram[m, 0] = hi
        gram[m, 1] = (g - hi.astype(F32)).astype(BF16)

    sq = {}
    for m in range(2):
        for q in range(1, ntp):
            sq[m, q] = Send(ss.at[m], ssg.at[m, q], ssg.at[m, q], along_x(q))

    def squares(m):
        dmo[m].arrived()
        for i in range(len(OFFSETS)):
            dm[m, i].arrived()
        d = dirg[m].reshape(R, C)
        e = jnp.dot(gram[m, 0], d, preferred_element_type=F32)
        e += jnp.dot(gram[m, 1], d, preferred_element_type=F32)
        p = jnp.sum((e * d.astype(F32)).reshape(R // 8, 8, C), axis=0)
        t = p[:, :128]
        for b in range(1, C // 128):
            t = t + p[:, b * 128:(b + 1) * 128]
        ss[m] = t
        for q in range(1, ntp):
            sq[m, q].start()
        o = pltpu.make_async_copy(dirg.at[m], dir_out.at[m], sem_out.at[4 + m])
        o.start()
        f_outs.append(o)

    def total(m):
        t = ss[m]
        for q in range(1, ntp):
            sq[m, q].arrived()
            t = t + ssg[m, q]
        ss_out[m] = t

    n_tiles = D // GN
    pl.semaphore_wait(barrier, len(OFFSETS) + 1 + ntp - 1)
    f_first(0)
    f_first(1)
    hooks = {
        (0, 1): lambda: f_second(0),
        (0, 2): lambda: f_second(1),
        (0, 3): lambda: w_first(),
        (1, 0): lambda: f_across(0, (1, 3)),
        (1, 1): lambda: f_across(0, (2,)),
        (1, 2): lambda: f_mate(0, (0,)),
        (1, 4): lambda: f_across(1, (1, 3)),
        (1, 5): lambda: (f_across(1, (2,)), w_second((0, 1))),
        (1, 6): lambda: f_mate(0, (1, 3)),
        (1, 7): lambda: (f_mate(0, (2,)), f_mate(1, (0,))),
    }
    for m in range(2):
        turn_cols(m)
        for n in range(n_tiles):
            gradient(m, n)
            if (m, n) in hooks:
                hooks[m, n]()
    f_done(0)
    project(0)
    f_mate(1, (1, 3))
    scatter(0)
    w_second((2,))
    gram_of(0)
    f_mate(1, (2,))
    f_done(1)
    project(1)
    moments(0, first_v, second_v, fnew_v, snew_v)
    scatter(1)
    w_second((3,))
    gram_of(1)
    spread(0)
    squares(0)
    w_mate((0,))
    moments(1, first_o, second_o, fnew_o, snew_o)
    w_mate((1, 3, 2))
    spread(1)
    squares(1)
    for g in range(NZ):
        for m in range(2):
            wm[m, g].arrived()
    for m in range(2):
        o = pltpu.make_async_copy(wg.at[m], wg_out.at[m], sem_out.at[2 + m])
        o.start()
        f_outs.append(o)
    total(0)
    total(1)
    for o in f_outs:
        o.wait()
    for p in pend:
        p.wait_send()


def finish_kernel(
    ntp,
    fg_in, wg_in, dir_in, ss_in, fac_v, fac_o, w_v, w_o, fn_v, sn_v, fn_o, sn_o,
    step_v, upd_v, fnew_v, snew_v, copy_v, step_o, upd_o, fnew_o, snew_o, copy_o,
    fg, wg, dirg, res, sem_f, sem_w, sem_d, sem_o,
):
    _, D, R = fg.shape
    C = wg.shape[2]
    CH = fg.shape[1] // sem_f.shape[1]
    n_ch = sem_f.shape[1]
    loads, outs = {}, []
    for m in range(2):
        loads["d", m] = pltpu.make_async_copy(dir_in.at[m], dirg.at[m], sem_d.at[m])
        loads["d", m].start()
        for b in range(n_ch):
            at = pl.ds(b * CH, CH)
            loads["f", m, b] = pltpu.make_async_copy(fg_in.at[m, at], fg.at[m, at], sem_f.at[m, b])
            loads["w", m, b] = pltpu.make_async_copy(wg_in.at[m, at], wg.at[m, at], sem_w.at[m, b])
            loads["f", m, b].start()
            loads["w", m, b].start()
    fnew_v[...] = fn_v[...]
    snew_v[...] = sn_v[...]
    fnew_o[...] = fn_o[...]
    snew_o[...] = sn_o[...]
    for m, (fac, w, step, upd, copy) in enumerate(
        ((fac_v, w_v, step_v, upd_v, copy_v), (fac_o, w_o, step_o, upd_o, copy_o))
    ):
        mean = jnp.sum(ss_in[m], keepdims=True) / (D * C * ntp)
        scale = step_rate / jnp.sqrt(mean + scale_floor)
        loads["d", m].wait()
        d = dirg[m]
        s = scale * jnp.dot(fac[...], d, preferred_element_type=F32)
        step[...] = s
        upd[...] = w[...] - s
        for b in range(n_ch):
            at = pl.ds(b * CH, CH)
            loads["f", m, b].wait()
            loads["w", m, b].wait()
            e = jnp.dot(fg[m, at], d, preferred_element_type=F32)
            res[m, at] = (wg[m, at].astype(F32) - scale * e).astype(BF16)
            o = pltpu.make_async_copy(res.at[m, at], copy.at[at], sem_o.at[m, b])
            o.start()
            outs.append(o)
    for o in outs:
        o.wait()


def local(
    n, ntp,
    model_input, value_cotan, mixer_cotan, head_output,
    value_weight, value_factor, value_first, value_second,
    output_weight, output_factor, output_first, output_second,
):
    T, D = model_input.shape
    C = value_cotan.shape[1]
    B, R = value_factor.shape
    k = value_first.shape[0]
    np_ = NZ * NZ
    vm = pl.BlockSpec(memory_space=pltpu.VMEM)
    hbm = pl.BlockSpec(memory_space=pl.ANY)
    mom = jax.ShapeDtypeStruct((k, C), F32)
    wide = jax.ShapeDtypeStruct((B, C), F32)
    full = jax.ShapeDtypeStruct((D, C), BF16)
    dma = pltpu.SemaphoreType.DMA
    fg_shape = (2, NZ, NZ, NC, NQ, B // NQ, R)
    wg_shape = (2, NZ, NZ, NC, WS, B // WS, C)
    dir_shape = (2, np_, NC, k, C)
    fn_v, sn_v, fn_o, sn_o, ss, fg, wg, dirg = pl.pallas_call(
        functools.partial(gather_kernel, ntp),
        out_shape=(mom,) * 4 + (
            jax.ShapeDtypeStruct((2, 8, 128), F32),
            jax.ShapeDtypeStruct(fg_shape, BF16),
            jax.ShapeDtypeStruct(wg_shape, BF16),
            jax.ShapeDtypeStruct(dir_shape, BF16),
        ),
        in_specs=[hbm] * 4 + [vm] * 8,
        out_specs=(vm,) * 5 + (hbm,) * 3,
        scratch_shapes=[
            pltpu.VMEM((2, T, D), BF16),
            pltpu.VMEM((2, T, C), BF16),
            pltpu.VMEM((2, C, T), BF16),
            pltpu.VMEM((2, C, D), BF16),
            pltpu.VMEM(fg_shape, BF16),
            pltpu.VMEM(wg_shape, BF16),
            pltpu.VMEM((2, np_, NC, k, C), F32),
            pltpu.VMEM((2, np_, k, C), BF16),
            pltpu.VMEM((2, np_, k, C), BF16),
            pltpu.VMEM((2, np_, k, C), BF16),
            pltpu.VMEM((2, np_ - 1, k, C), BF16),
            pltpu.VMEM((2, k, C), F32),
            pltpu.VMEM(dir_shape, BF16),
            pltpu.VMEM((2, 2, R, R), BF16),
            pltpu.VMEM((2, 8, 128), F32),
            pltpu.VMEM((2, ntp, 8, 128), F32),
            dma((2, 4)), dma((2,)), dma((6,)), dma((N_SEMS,)), dma((N_SEMS,)),
        ],
        compiler_params=pltpu.CompilerParams(
            collective_id=0, has_side_effects=True, vmem_limit_bytes=62_000_000
        ),
        name="gather",
    )(
        model_input, value_cotan, mixer_cotan, head_output,
        value_factor, output_factor, value_weight, output_weight,
        value_first, output_first, value_second, output_second,
    )
    n_ch = 4
    return pl.pallas_call(
        functools.partial(finish_kernel, ntp),
        out_shape=(wide, wide, mom, mom, full) * 2,
        in_specs=[hbm] * 3 + [vm] * 9,
        out_specs=(vm, vm, vm, vm, hbm) * 2,
        scratch_shapes=[
            pltpu.VMEM((2, D, R), BF16),
            pltpu.VMEM((2, D, C), BF16),
            pltpu.VMEM((2, R, C), BF16),
            pltpu.VMEM((2, D, C), BF16),
            dma((2, n_ch)), dma((2, n_ch)), dma((2,)), dma((2, n_ch)),
        ],
        compiler_params=pltpu.CompilerParams(vmem_limit_bytes=62_000_000),
        name="finish",
    )(
        fg.reshape(2, D, R), wg.reshape(2, D, C), dirg.reshape(2, R, C), ss,
        value_factor, output_factor, value_weight, output_weight,
        fn_v, sn_v, fn_o, sn_o,
    )


def solution(mesh):
    rows, both, full = P("fs", None), P("fs", "tp"), P(None, "tp")
    return jax.shard_map(
        functools.partial(local, mesh.shape["fs"], mesh.shape["tp"]),
        mesh=mesh,
        in_specs=(rows, both, rows, both) + (both, rows, both, both) * 2,
        out_specs=(both, both, both, both, full) * 2,
        check_vma=False,
    )
```

time: 166 us -> 76.2 us (0.46)
  Pallas kernels: 151 us -> 75.2 us
  local copies, waits for them, and re-layouts: 13 us -> 0 us
    pallas_call x1 -> x2, Pallas kernels: 151 us -> 75.2 us  [the longest x1 65 us: local(): pl.pallas_call(functools.partial(gather_kernel, ntp), out_shape=(mom,) *...]
    unnamed x20 -> x0, local copies, waits for them, and re-layouts: 13 us -> none
where the time goes in v1:
time: 76.2 us; the launch traced here: 76 us
  Pallas kernels  75.2 us (99%)
  between operations  0.81 us (1%)
    pallas_call x1, Pallas kernels, local(): pl.pallas_call(functools.partial(gather_kernel, ntp), out_shape=(mom,) *...  65 us
    pallas_call x1, Pallas kernels, local(): pl.pallas_call(functools.partial(finish_kernel, ntp), out_shape=(wide, wi...  10.2 us

profile of v1, /device:TPU:1, one launch (start us, length us, event | category | flops | bytes accessed | tf_op | source)
XLA Modules:
  0.0 76.0 jit_solution(13536988262656577597)
XLA Ops:
  0.6 65.0 %gather.1 = (f32[16,512]{1,0:T(8,128)}, f32[16,512]{1,0:T(8,128)}, f32[16,512]{1,0:T(8,128)}, f32[16,512]{1,0:T(8,128)}, f32[2,8,128]{2,1,0:T(8,128)}, /*index=5...) custom-call(bf16[2048,2048]{1,0:T(8,128)(2,1)} %rows_v.1, ...), custom_call_target="tpu_custom_call" | custom-call | tf_op jit(solution)/shard_map/gather/pallas_call | solution.py:442
  65.7 10.2 %finish.1 = (f32[64,512]{1,0:T(8,128)}, f32[64,512]{1,0:T(8,128)}, f32[16,512]{1,0:T(8,128)}, f32[16,512]{1,0:T(8,128)}, bf16[2048,512]{1,0:T(8,128)(2,1)}, /*in...) custom-call(bf16[2,2048,512]{2,1,0:T(8,128)(2,1)} %bitcast.3, ...), custom_call_target="tpu_custom_call" | custom-call | tf_op jit(solution)/shard_map/finish/pallas_call | solution.py:481

commit v2 on v1

v2 whole, which is shorter than its diff:
```python
import functools
import math

import jax
import jax.numpy as jnp
from jax import lax
from jax.experimental import pallas as pl
from jax.experimental.pallas import tpu as pltpu
from jax.sharding import PartitionSpec as P

beta_first = 0.8
beta_second = 0.9
step_rate = 0.02
scale_floor = 0.25
tiny_eps = 1e-08

MESH = pl.DeviceIdType.MESH
F32 = jnp.float32
BF16 = jnp.bfloat16
NZ = 4
NC = 2
NQ = 4
WS = 4
N_SEMS = 40
OFFSETS = sorted(
    [(a, b) for a in range(NZ) for b in range(NZ) if a or b],
    key=lambda o: -(min(o[0], NZ - o[0]) + min(o[1], NZ - o[1])),
)


def gather_kernel(
    ntp,
    rows_v, cols_v, rows_o, cols_o,
    fac_v, fac_o, w_v, w_o, first_v, first_o, second_v, second_o,
    fnew_v, snew_v, fnew_o, snew_o, ss_out, fg_out, wg_out, dir_out,
    rows, cols, cols_t, grad, fg, wg, pf, send_a, recv_a, send_b, recv_b, pg,
    dirg, gram, ss, ssg, sst, tally, wide, old, new,
    sem_rows, sem_cols, sem_out, sem_in, sem_new, ssem, rsem,
):
    me = lax.axis_index("fs")
    tp = lax.axis_index("tp")
    z, y, c = me // (NZ * NC), lax.rem(me // NC, NZ), lax.rem(me, NC)
    co = 1 - c
    chip = z * NZ + y
    h = lax.rem(tp, 2)
    T, D = rows_v.shape
    C = cols_v.shape[1]
    QR, R = fac_v.shape[1:]
    WR = w_v.shape[0] // WS

    def up(a, d):
        return lax.rem(a + d, NZ)

    def dn(a, d):
        return lax.rem(a + NZ - d, NZ)

    def plane(zz, yy):
        return ((zz * NZ + yy) * NC + c, tp)

    mate = (me - c + co, tp)

    def along_x(d):
        return (me, lax.rem(tp + ntp + d, ntp))

    row_bytes = 2 * tally.shape[1] * tally.shape[2]
    n_recv = [0]
    out_bytes = [0]

    def size(ref):
        return math.prod(ref.shape) * jnp.dtype(ref.dtype).itemsize // row_bytes

    class Group:
        def __init__(self):
            self.i, self.rows = n_recv[0], 0
            n_recv[0] += 1

        def arrived(self):
            all_of = tally.at[pl.ds(0, self.rows)]
            pltpu.make_async_remote_copy(
                src_ref=all_of, dst_ref=all_of, send_sem=ssem.at[0], recv_sem=rsem.at[self.i],
                device_id=mate, device_id_type=MESH,
            ).wait_recv()

    class Send:
        def __init__(self, src, dst, group, dev):
            if out_bytes[-1] + size(src) > tally.shape[0]:
                out_bytes.append(0)
            out_bytes[-1] += size(src)
            group.rows += size(src)
            self.copy = pltpu.make_async_remote_copy(
                src_ref=src, dst_ref=dst, send_sem=ssem.at[len(out_bytes) - 1], recv_sem=rsem.at[group.i],
                device_id=dev, device_id_type=MESH,
            )

        def start(self):
            self.copy.start()

    barrier = pltpu.get_barrier_semaphore()
    for dz, dy in OFFSETS:
        pl.semaphore_signal(barrier, inc=1, device_id=plane(up(z, dz), up(y, dy)), device_id_type=MESH)
    pl.semaphore_signal(barrier, inc=1, device_id=mate, device_id_type=MESH)
    for q in range(1, ntp):
        pl.semaphore_signal(barrier, inc=1, device_id=along_x(q), device_id_type=MESH)

    half = D // 4
    f_loads, w_loads, o_loads, row_loads, col_loads = [], [], [], [[], []], []
    for m, (r, cc, f, w, a, b) in enumerate((
        (rows_v, cols_v, fac_v, w_v, first_v, second_v), (rows_o, cols_o, fac_o, w_o, first_o, second_o)
    )):
        mine = pl.ds(2 * h, 2)
        f_loads.append(pltpu.make_async_copy(f.at[mine], fg.at[m, z, y, c, mine], sem_in.at[m]))
        w_loads.append(pltpu.make_async_copy(w, wide.at[m], sem_in.at[2 + m]))
        o_loads.append(pltpu.make_async_copy(a, old.at[m, 0], sem_in.at[4 + m]))
        o_loads.append(pltpu.make_async_copy(b, old.at[m, 1], sem_in.at[6 + m]))
        col_loads.append(pltpu.make_async_copy(cc, cols.at[m], sem_cols.at[m]))
        for j in range(4):
            at = pl.ds(j * half, half)
            row_loads[m].append(pltpu.make_async_copy(r.at[:, at], rows.at[m, :, at], sem_rows.at[m, j]))
    for x in (*f_loads, *w_loads, col_loads[0], row_loads[0][0], row_loads[0][1]):
        x.start()

    def line(buf, m, s, g, cc, k):
        return buf.at[m, :, dn(y, g), cc, k] if s == 0 else buf.at[m, dn(z, g), :, cc, k]

    def own(buf, m, s, d, k):
        return buf.at[m, dn(z, d), y, c, k] if s == 0 else buf.at[m, z, dn(y, d), c, k]

    def first_dev(s, d):
        return plane(up(z, d), y) if s == 0 else plane(z, up(y, d))

    def second_dev(s, d):
        return plane(z, up(y, d)) if s == 0 else plane(up(z, d), y)

    f1, f2, fx, fm, fxm = {}, {}, {}, {}, {}
    f1_in, f2_in, fx_in, fm_in = {}, {}, {}, {}
    for m in range(2):
        f1_in[m], fm_in[m] = Group(), Group()
        f2_in[m, 1] = f2_in[m, 3] = Group()
        f2_in[m, 2] = Group()
        fx_in[m, 0], fx_in[m, 2] = Group(), Group()
        fx_in[m, 1] = fx_in[m, 3] = Group()
        for s in range(2):
            k, kx = 2 * h + s, 2 * (1 - h) + s
            for d in (2, 1, 3):
                f1[m, s, d] = Send(own(fg, m, s, 0, k), own(fg, m, s, 0, k), f1_in[m], first_dev(s, d))
                f2[m, s, d] = Send(line(fg, m, s, 0, c, k), line(fg, m, s, 0, c, k), f2_in[m, d], second_dev(s, d))
            for g in range(NZ):
                a, b = line(fg, m, s, g, c, k), line(fg, m, s, g, c, kx)
                fx[m, s, g] = Send(a, a, fx_in[m, g], along_x(1 if s == 0 else -1))
                fm[m, s, g] = Send(a, a, fm_in[m], mate)
                fxm[m, s, g] = Send(b, b, fm_in[m], mate)

    def f_first(m):
        for d in (2, 1, 3):
            for s in range(2):
                f1[m, s, d].start()

    def f_second(m):
        f1_in[m].arrived()
        for d in (1, 3, 2):
            for s in range(2):
                f2[m, s, d].start()
        for s in range(2):
            fx[m, s, 0].start()
            fm[m, s, 0].start()

    def f_across(m, gs):
        f2_in[m, gs[0]].arrived()
        for g in gs:
            for s in range(2):
                fx[m, s, g].start()
                fm[m, s, g].start()

    def f_mate(m, gs):
        fx_in[m, gs[0]].arrived()
        for g in gs:
            for s in range(2):
                fxm[m, s, g].start()

    f_outs = []

    def f_done(m):
        fm_in[m].arrived()
        o = pltpu.make_async_copy(fg.at[m], fg_out.at[m], sem_out.at[m])
        o.start()
        f_outs.append(o)

    w1, w2, w3, wm = {}, {}, {}, {}

    def part(m, j, g, b):
        two = pl.ds(2 * b, 2)
        return wg.at[m, two, dn(y, g), c, j] if m == 0 else wg.at[m, dn(z, g), two, c, j]

    w1_in, w3_in, wm_in = Group(), Group(), Group()
    w2_in = {}
    for j in range(WS):
        w2_in[j] = Group()
        for m in range(2):
            for d in (2, 1, 3):
                w1[m, j, d] = Send(own(wg, m, m, 0, j), own(wg, m, m, 0, j), w1_in, first_dev(m, d))
            for d in (1, 3):
                w2[m, j, d] = Send(line(wg, m, m, 0, c, j), line(wg, m, m, 0, c, j), w2_in[j], second_dev(m, d))
                b = d // 2
                w3[m, j, d] = Send(part(m, j, d, b), part(m, j, d, b), w3_in, second_dev(m, d))
    for m in range(2):
        for g in range(NZ):
            a = wg.at[m, :, dn(y, g), c] if m == 0 else wg.at[m, dn(z, g), :, c]
            wm[m, g] = Send(a, a, wm_in, mate)

    def w_own():
        for m in range(2):
            w_loads[m].wait()
            wg[m, z, y, c] = wide[m].reshape(WS, WR, C).astype(BF16)

    def w_first():
        for j in range(WS):
            for d in (2, 1, 3):
                for m in range(2):
                    w1[m, j, d].start()

    def w_second(js):
        if js[0] == 0:
            w1_in.arrived()
        for j in js:
            for d in (1, 3):
                for m in range(2):
                    w2[m, j, d].start()

    def w_third(js):
        for j in js:
            w2_in[j].arrived()
            for d in (1, 3):
                for m in range(2):
                    w3[m, j, d].start()

    def w_mate(gs):
        if gs[0] == 2:
            w3_in.arrived()
        for g in gs:
            for m in range(2):
                wm[m, g].start()

    def turn_cols(m):
        col_loads[m].wait()
        for t in range(4):
            at = pl.ds(t * (T // 4), T // 4)
            cols_t[m, :, at] = cols[m, at, :].T

    def gradient(m, n):
        j, b = n // 2, n % 2
        if b == 0:
            row_loads[m][j].wait()
        at, up_to = pl.ds(j * half, half), pl.ds(b * (C // 2), C // 2)
        grad[m, up_to, at] = jnp.dot(cols_t[m, up_to], rows[m, :, at], preferred_element_type=F32).astype(BF16)

    def factor_of(m):
        return fg[m].reshape(D, R)

    sa, sb, sa_in, sb_in = {}, {}, {}, {}
    for m in range(2):
        sa_in[m], sb_in[m] = Group(), Group()
        sa[m] = Send(send_a.at[m], recv_a.at[m], sa_in[m], mate)
        for i, (dz, dy) in enumerate(OFFSETS):
            to = up(z, dz) * NZ + up(y, dy)
            sb[m, i] = Send(send_b.at[m, to], recv_b.at[m, i], sb_in[m], plane(up(z, dz), up(y, dy)))

    def project(m):
        pt = jnp.dot(grad[m], factor_of(m), preferred_element_type=F32)
        pf[m] = pt.T.reshape(NZ * NZ, NC, QR, C)
        send_a[m] = pf[m, :, co].astype(BF16)
        sa[m].start()

    def scatter(m):
        sa_in[m].arrived()
        send_b[m] = (pf[m, :, c] + recv_a[m].astype(F32)).astype(BF16)
        for i in range(len(OFFSETS)):
            sb[m, i].start()
        pg[m] = pf[m, chip, c] + recv_a[m, chip].astype(F32)

    dp, dm, dp_in, dm_in = {}, {}, {}, {}
    for m in range(2):
        dp_in[m], dm_in[m] = Group(), Group()
        mine = dirg.at[m, chip, c]
        for i, (dz, dy) in enumerate(OFFSETS):
            dp[m, i] = Send(mine, mine, dp_in[m], plane(up(z, dz), up(y, dy)))
        dm[m] = Send(dirg.at[m, :, c], dirg.at[m, :, c], dm_in[m], mate)

    def moments(m, fnew, snew):
        tot = pg[m]
        o_loads[2 * m].wait()
        o_loads[2 * m + 1].wait()
        sb_in[m].arrived()
        for i in range(len(OFFSETS)):
            tot = tot + recv_b[m, i].astype(F32)
        f = beta_first * old[m, 0] + (1.0 - beta_first) * tot
        s = beta_second * old[m, 1] + (1.0 - beta_second) * tot * tot
        dirg[m, chip, c] = (f / (jnp.sqrt(s) + tiny_eps)).astype(BF16)
        for i in range(len(OFFSETS)):
            dp[m, i].start()
        new[m, 0] = f
        new[m, 1] = s
        for i, out in enumerate((fnew, snew)):
            o = pltpu.make_async_copy(new.at[m, i], out, sem_new.at[m, i])
            o.start()
            f_outs.append(o)

    def spread(m):
        dp_in[m].arrived()
        dm[m].start()

    def gram_of(m):
        f = factor_of(m)
        ft = f.T
        g = jnp.dot(ft, f, preferred_element_type=F32)
        hi = g.astype(BF16)
        gram[m, 0] = hi
        gram[m, 1] = (g - hi.astype(F32)).astype(BF16)

    sq, sq_in = {}, {}
    for m in range(2):
        sq_in[m] = Group()
        for q in range(1, ntp):
            sq[m, q] = Send(ss.at[m], ssg.at[m, q], sq_in[m], along_x(q))

    def squares(m):
        dm_in[m].arrived()
        d = dirg[m].reshape(R, C)
        e = jnp.dot(gram[m, 0], d, preferred_element_type=F32)
        e += jnp.dot(gram[m, 1], d, preferred_element_type=F32)
        p = jnp.sum((e * d.astype(F32)).reshape(R // 8, 8, C), axis=0)
        t = p[:, :128]
        for b in range(1, C // 128):
            t = t + p[:, b * 128:(b + 1) * 128]
        ss[m] = t
        for q in range(1, ntp):
            sq[m, q].start()
        o = pltpu.make_async_copy(dirg.at[m], dir_out.at[m], sem_out.at[4 + m])
        o.start()
        f_outs.append(o)

    def total(m):
        t = ss[m]
        sq_in[m].arrived()
        for q in range(1, ntp):
            t = t + ssg[m, q]
        sst[m] = t
        o = pltpu.make_async_copy(sst.at[m], ss_out.at[m], sem_new.at[m, 2])
        o.start()
        f_outs.append(o)

    for x in f_loads:
        x.wait()
    pl.semaphore_wait(barrier, len(OFFSETS) + 1 + ntp - 1)
    f_first(0)
    f_first(1)
    w_own()
    w_first()
    for x in (row_loads[0][2], row_loads[0][3], col_loads[1], *o_loads):
        x.start()

    def more_rows():
        for x in row_loads[1]:
            x.start()

    hooks = {
        (0, 1): lambda: (more_rows(), f_second(0)),
        (0, 2): lambda: f_second(1),
        (0, 3): lambda: w_second(range(WS)),
        (0, 7): lambda: f_across(0, (1, 3)),
        (1, 0): lambda: (f_across(0, (2,)), f_mate(0, (0,))),
        (1, 2): lambda: (f_across(1, (1, 3)), f_mate(1, (0,))),
        (1, 4): lambda: (f_mate(0, (1, 3)), f_across(1, (2,))),
        (1, 6): lambda: (f_mate(0, (2,)), w_third((0, 1))),
        (1, 7): lambda: f_mate(1, (1, 3)),
    }
    for m in range(2):
        turn_cols(m)
        for n in range(8):
            gradient(m, n)
            if (m, n) in hooks:
                hooks[m, n]()
    f_done(0)
    project(0)
    f_mate(1, (2,))
    w_third((2, 3))
    scatter(0)
    f_done(1)
    project(1)
    gram_of(0)
    scatter(1)
    moments(0, fnew_v, snew_v)
    w_mate((0, 1, 3))
    gram_of(1)
    spread(0)
    moments(1, fnew_o, snew_o)
    squares(0)
    w_mate((2,))
    spread(1)
    squares(1)
    wm_in.arrived()
    for m in range(2):
        o = pltpu.make_async_copy(wg.at[m], wg_out.at[m], sem_out.at[2 + m])
        o.start()
        f_outs.append(o)
    total(0)
    total(1)
    for o in f_outs:
        o.wait()
    for i, n in enumerate(out_bytes):
        all_of = tally.at[pl.ds(0, n)]
        pltpu.make_async_remote_copy(
            src_ref=all_of, dst_ref=all_of, send_sem=ssem.at[i], recv_sem=rsem.at[0],
            device_id=mate, device_id_type=MESH,
        ).wait_send()


def finish_kernel(
    ntp,
    fg_in, wg_in, dir_in, ss_in, fac_v, fac_o, w_v, w_o, fn_v, sn_v, fn_o, sn_o,
    step_v, upd_v, fnew_v, snew_v, copy_v, step_o, upd_o, fnew_o, snew_o, copy_o,
    fg, wg, dirg, res, fac, w, mo, ss, st, up, sem_f, sem_w, sem_s, sem_o, sem_p,
):
    _, D, R = fg.shape
    C = wg.shape[2]
    n_ch = sem_f.shape[1]
    CH = D // n_ch
    loads, outs = {}, []

    def load(key, src, dst, sem):
        loads[key] = pltpu.make_async_copy(src, dst, sem)
        loads[key].start()

    def store(src, dst, sem):
        o = pltpu.make_async_copy(src, dst, sem)
        o.start()
        outs.append(o)

    load("s", ss_in, ss, sem_s.at[0])
    mo_out = ((fnew_v, snew_v), (fnew_o, snew_o))
    for m in range(2):
        load(("d", m), dir_in.at[m], dirg.at[m], sem_s.at[1 + m])
        for b in range(n_ch):
            at = pl.ds(b * CH, CH)
            load(("f", m, b), fg_in.at[m, at], fg.at[m, at], sem_f.at[m, b])
            load(("w", m, b), wg_in.at[m, at], wg.at[m, at], sem_w.at[m, b])
        load(("k", m), (fac_v, fac_o)[m], fac.at[m], sem_s.at[3 + m])
        load(("g", m), (w_v, w_o)[m], w.at[m], sem_s.at[5 + m])
        for i in range(2):
            load(("m", m, i), ((fn_v, sn_v), (fn_o, sn_o))[m][i], mo.at[m, i], sem_p.at[m, i])
    loads["s"].wait()
    for m, (step, upd, copy) in enumerate(((step_v, upd_v, copy_v), (step_o, upd_o, copy_o))):
        mean = jnp.sum(ss[m], keepdims=True) / (D * C * ntp)
        scale = step_rate / jnp.sqrt(mean + scale_floor)
        loads["d", m].wait()
        d = dirg[m]
        for b in range(n_ch):
            at = pl.ds(b * CH, CH)
            loads["f", m, b].wait()
            loads["w", m, b].wait()
            with jax.named_scope(f"fin_{m}_{b}"):
                e = jnp.dot(fg[m, at], d, preferred_element_type=F32)
                res[m, at] = (wg[m, at].astype(F32) - scale * e).astype(BF16)
            store(res.at[m, at], copy.at[at], sem_o.at[m, b])
        for i in range(2):
            loads["m", m, i].wait()
            store(mo.at[m, i], mo_out[m][i], sem_p.at[m, i])
        loads["k", m].wait()
        loads["g", m].wait()
        s = scale * jnp.dot(fac[m], d, preferred_element_type=F32)
        st[m] = s
        up[m] = w[m] - s
        store(st.at[m], step, sem_s.at[7 + m])
        store(up.at[m], upd, sem_s.at[9 + m])
    for o in outs:
        o.wait()


def local(
    n, ntp,
    model_input, value_cotan, mixer_cotan, head_output,
    value_weight, value_factor, value_first, value_second,
    output_weight, output_factor, output_first, output_second,
):
    T, D = model_input.shape
    C = value_cotan.shape[1]
    B, R = value_factor.shape
    k = value_first.shape[0]
    np_ = NZ * NZ
    hbm = pl.BlockSpec(memory_space=pl.ANY)
    mom = jax.ShapeDtypeStruct((k, C), F32)
    wide = jax.ShapeDtypeStruct((B, C), F32)
    full = jax.ShapeDtypeStruct((D, C), BF16)
    dma = pltpu.SemaphoreType.DMA
    fg_shape = (2, NZ, NZ, NC, NQ, B // NQ, R)
    wg_shape = (2, NZ, NZ, NC, WS, B // WS, C)
    dir_shape = (2, np_, NC, k, C)
    fn_v, sn_v, fn_o, sn_o, ss, fg, wg, dirg = pl.pallas_call(
        functools.partial(gather_kernel, ntp),
        out_shape=(mom,) * 4 + (
            jax.ShapeDtypeStruct((2, 8, 128), F32),
            jax.ShapeDtypeStruct(fg_shape, BF16),
            jax.ShapeDtypeStruct(wg_shape, BF16),
            jax.ShapeDtypeStruct(dir_shape, BF16),
        ),
        in_specs=[hbm] * 12,
        out_specs=(hbm,) * 8,
        scratch_shapes=[
            pltpu.VMEM((2, T, D), BF16),
            pltpu.VMEM((2, T, C), BF16),
            pltpu.VMEM((2, C, T), BF16),
            pltpu.VMEM((2, C, D), BF16),
            pltpu.VMEM(fg_shape, BF16),
            pltpu.VMEM(wg_shape, BF16),
            pltpu.VMEM((2, np_, NC, k, C), F32),
            pltpu.VMEM((2, np_, k, C), BF16),
            pltpu.VMEM((2, np_, k, C), BF16),
            pltpu.VMEM((2, np_, k, C), BF16),
            pltpu.VMEM((2, np_ - 1, k, C), BF16),
            pltpu.VMEM((2, k, C), F32),
            pltpu.VMEM(dir_shape, BF16),
            pltpu.VMEM((2, 2, R, R), BF16),
            pltpu.VMEM((2, 8, 128), F32),
            pltpu.VMEM((2, ntp, 8, 128), F32),
            pltpu.VMEM((2, 8, 128), F32),
            pltpu.VMEM((512, 16, 128), BF16),
            pltpu.VMEM((2, B, C), F32),
            pltpu.VMEM((2, 2, k, C), F32),
            pltpu.VMEM((2, 2, k, C), F32),
            dma((2, 4)), dma((2,)), dma((6,)), dma((8,)), dma((2, 3)), dma((N_SEMS,)), dma((N_SEMS,)),
        ],
        compiler_params=pltpu.CompilerParams(
            collective_id=0, has_side_effects=True, vmem_limit_bytes=62_000_000
        ),
        name="gather",
    )(
        model_input, value_cotan, mixer_cotan, head_output,
        value_factor.reshape(NQ, B // NQ, R), output_factor.reshape(NQ, B // NQ, R), value_weight, output_weight,
        value_first, output_first, value_second, output_second,
    )
    n_ch = 4
    return pl.pallas_call(
        functools.partial(finish_kernel, ntp),
        out_shape=(wide, wide, mom, mom, full) * 2,
        in_specs=[hbm] * 12,
        out_specs=(hbm,) * 10,
        scratch_shapes=[
            pltpu.VMEM((2, D, R), BF16),
            pltpu.VMEM((2, D, C), BF16),
            pltpu.VMEM((2, R, C), BF16),
            pltpu.VMEM((2, D, C), BF16),
            pltpu.VMEM((2, B, R), BF16),
            pltpu.VMEM((2, B, C), F32),
            pltpu.VMEM((2, 2, k, C), F32),
            pltpu.VMEM((2, 8, 128), F32),
            pltpu.VMEM((2, B, C), F32),
            pltpu.VMEM((2, B, C), F32),
            dma((2, n_ch)), dma((2, n_ch)), dma((11,)), dma((2, n_ch)), dma((2, 2)),
        ],
        compiler_params=pltpu.CompilerParams(vmem_limit_bytes=62_000_000),
        name="finish",
    )(
        fg.reshape(2, D, R), wg.reshape(2, D, C), dirg.reshape(2, R, C), ss,
        value_factor, output_factor, value_weight, output_weight,
        fn_v, sn_v, fn_o, sn_o,
    )


def solution(mesh):
    rows, both, full = P("fs", None), P("fs", "tp"), P(None, "tp")
    return jax.shard_map(
        functools.partial(local, mesh.shape["fs"], mesh.shape["tp"]),
        mesh=mesh,
        in_specs=(rows, both, rows, both) + (both, rows, both, both) * 2,
        out_specs=(both, both, both, both, full) * 2,
        check_vma=False,
    )
```

time: 76.2 us -> 61.6 us (0.81)
  Pallas kernels: 75.2 us -> 60.7 us
    pallas_call x1, Pallas kernels: 65 us -> 53.8 us  [local(): pl.pallas_call(functools.partial(gather_kernel, ntp), out_shape=(mom,) *...]
    pallas_call x1, Pallas kernels: 10.2 us -> 6.88 us  [local(): pl.pallas_call(functools.partial(finish_kernel, ntp), out_shape=(wide, wi...]
where the time goes in v2:
time: 61.6 us; the launch traced here: 61.5 us
  Pallas kernels  60.7 us (99%)
  between operations  0.81 us (1%)
    pallas_call x1, Pallas kernels, local(): pl.pallas_call(functools.partial(gather_kernel, ntp), out_shape=(mom,) *...  53.8 us
    pallas_call x1, Pallas kernels, local(): pl.pallas_call(functools.partial(finish_kernel, ntp), out_shape=(wide, wi...  6.88 us

profile of v2, /device:TPU:1, one launch (start us, length us, event | category | flops | bytes accessed | tf_op | source)
XLA Modules:
  0.0 61.5 jit_solution(309501997147308466)
XLA Ops:
  0.6 53.8 %gather.1 = (f32[16,512]{1,0:T(8,128)}, f32[16,512]{1,0:T(8,128)}, f32[16,512]{1,0:T(8,128)}, f32[16,512]{1,0:T(8,128)}, f32[2,8,128]{2,1,0:T(8,128)}, /*index=5...) custom-call(bf16[2048,2048]{1,0:T(8,128)(2,1)} %rows_v.1, ...), custom_call_target="tpu_custom_call" | custom-call | tf_op jit(solution)/shard_map/gather/pallas_call | solution.py:497
  54.4 6.9 %finish.1 = (f32[64,512]{1,0:T(8,128)}, f32[64,512]{1,0:T(8,128)}, f32[16,512]{1,0:T(8,128)}, f32[16,512]{1,0:T(8,128)}, bf16[2048,512]{1,0:T(8,128)(2,1)}, /*in...) custom-call(bf16[2,2048,512]{2,1,0:T(8,128)(2,1)} %bitcast.5, ...), custom_call_target="tpu_custom_call" | custom-call | tf_op jit(solution)/shard_map/finish/pallas_call | solution.py:541

commit v3 on v2

--- a/solution.py
+++ b/solution.py
@@ -21,7 +21,8 @@
 NC = 2
 NQ = 4
 WS = 4
-N_SEMS = 40
+NH = 2
+N_SEMS = 64
 OFFSETS = sorted(
     [(a, b) for a in range(NZ) for b in range(NZ) if a or b],
     key=lambda o: -(min(o[0], NZ - o[0]) + min(o[1], NZ - o[1])),
@@ -32,10 +33,10 @@
     ntp,
     rows_v, cols_v, rows_o, cols_o,
     fac_v, fac_o, w_v, w_o, first_v, first_o, second_v, second_o,
-    fnew_v, snew_v, fnew_o, snew_o, ss_out, fg_out, wg_out, dir_out,
-    rows, cols, cols_t, grad, fg, wg, pf, send_a, recv_a, send_b, recv_b, pg,
-    dirg, gram, ss, ssg, sst, tally, wide, old, new,
-    sem_rows, sem_cols, sem_out, sem_in, sem_new, ssem, rsem,
+    new, sst, wg, ex,
+    rows, cols, cols_t, grad, fg, pf, send_a, recv_a, send_b, recv_b, pg,
+    dirg, gram, ss, ssg, tally, wide, old,
+    sem_rows, sem_cols, sem_in, ssem, rsem,
 ):
     me = lax.axis_index("fs")
     tp = lax.axis_index("tp")
@@ -146,7 +147,11 @@
                 f2[m, s, d] = Send(line(fg, m, s, 0, c, k), line(fg, m, s, 0, c, k), f2_in[m, d], second_dev(s, d))
             for g in range(NZ):
                 a, b = line(fg, m, s, g, c, k), line(fg, m, s, g, c, kx)
-                fx[m, s, g] = Send(a, a, fx_in[m, g], along_x(1 if s == 0 else -1))
+                if g == 2:
+                    o = line(fg, m, s, 0, c, kx)
+                    fx[m, s, g] = Send(o, o, fx_in[m, g], second_dev(s, 2))
+                else:
+                    fx[m, s, g] = Send(a, a, fx_in[m, g], along_x(1 if s == 0 else -1))
                 fm[m, s, g] = Send(a, a, fm_in[m], mate)
                 fxm[m, s, g] = Send(b, b, fm_in[m], mate)
 
@@ -168,22 +173,20 @@
         f2_in[m, gs[0]].arrived()
         for g in gs:
             for s in range(2):
-                fx[m, s, g].start()
+                if g != 2:
+                    fx[m, s, g].start()
                 fm[m, s, g].start()
 
     def f_mate(m, gs):
         fx_in[m, gs[0]].arrived()
         for g in gs:
             for s in range(2):
+                if g == 0:
+                    fx[m, s, 2].start()
                 fxm[m, s, g].start()
-
-    f_outs = []
 
     def f_done(m):
         fm_in[m].arrived()
-        o = pltpu.make_async_copy(fg.at[m], fg_out.at[m], sem_out.at[m])
-        o.start()
-        f_outs.append(o)
 
     w1, w2, w3, wm = {}, {}, {}, {}
 
@@ -226,9 +229,12 @@
                 for m in range(2):
                     w2[m, j, d].start()
 
+    def w_have(js):
+        for j in js:
+            w2_in[j].arrived()
+
     def w_third(js):
         for j in js:
-            w2_in[j].arrived()
             for d in (1, 3):
                 for m in range(2):
                     w3[m, j, d].start()
@@ -256,57 +262,58 @@
     def factor_of(m):
         return fg[m].reshape(D, R)
 
+    CW = C // NH
     sa, sb, sa_in, sb_in = {}, {}, {}, {}
+    dp, dp_in, dm, dm_in = {}, {}, {}, {}
     for m in range(2):
-        sa_in[m], sb_in[m] = Group(), Group()
-        sa[m] = Send(send_a.at[m], recv_a.at[m], sa_in[m], mate)
-        for i, (dz, dy) in enumerate(OFFSETS):
-            to = up(z, dz) * NZ + up(y, dy)
-            sb[m, i] = Send(send_b.at[m, to], recv_b.at[m, i], sb_in[m], plane(up(z, dz), up(y, dy)))
-
-    def project(m):
-        pt = jnp.dot(grad[m], factor_of(m), preferred_element_type=F32)
-        pf[m] = pt.T.reshape(NZ * NZ, NC, QR, C)
-        send_a[m] = pf[m, :, co].astype(BF16)
-        sa[m].start()
-
-    def scatter(m):
-        sa_in[m].arrived()
-        send_b[m] = (pf[m, :, c] + recv_a[m].astype(F32)).astype(BF16)
+        for b in range(NH):
+            p = m, b
+            sa_in[p], sb_in[p], dp_in[p], dm_in[p] = Group(), Group(), Group(), Group()
+            sa[p] = Send(send_a.at[m, b], recv_a.at[m, b], sa_in[p], mate)
+            mine = dirg.at[m, b, chip, c]
+            for i, (dz, dy) in enumerate(OFFSETS):
+                to = up(z, dz) * NZ + up(y, dy)
+                dev = plane(up(z, dz), up(y, dy))
+                sb[m, b, i] = Send(send_b.at[m, b, to], recv_b.at[m, b, i], sb_in[p], dev)
+                dp[m, b, i] = Send(mine, mine, dp_in[p], dev)
+            dm[p] = Send(dirg.at[m, b, :, c], dirg.at[m, b, :, c], dm_in[p], mate)
+
+    def project(m, b):
+        pt = jnp.dot(grad[m, pl.ds(b * CW, CW)], factor_of(m), preferred_element_type=F32)
+        pf[m, b] = pt.T.reshape(NZ * NZ, NC, QR, CW)
+        send_a[m, b] = pf[m, b, :, co].astype(BF16)
+        sa[m, b].start()
+
+    def scatter(m, b):
+        sa_in[m, b].arrived()
+        send_b[m, b] = (pf[m, b, :, c] + recv_a[m, b].astype(F32)).astype(BF16)
         for i in range(len(OFFSETS)):
-            sb[m, i].start()
-        pg[m] = pf[m, chip, c] + recv_a[m, chip].astype(F32)
-
-    dp, dm, dp_in, dm_in = {}, {}, {}, {}
-    for m in range(2):
-        dp_in[m], dm_in[m] = Group(), Group()
-        mine = dirg.at[m, chip, c]
-        for i, (dz, dy) in enumerate(OFFSETS):
-            dp[m, i] = Send(mine, mine, dp_in[m], plane(up(z, dz), up(y, dy)))
-        dm[m] = Send(dirg.at[m, :, c], dirg.at[m, :, c], dm_in[m], mate)
-
-    def moments(m, fnew, snew):
-        tot = pg[m]
-        o_loads[2 * m].wait()
-        o_loads[2 * m + 1].wait()
-        sb_in[m].arrived()
+            sb[m, b, i].start()
+        pg[m, b] = pf[m, b, chip, c] + recv_a[m, b, chip].astype(F32)
+
+    def moments(m, b):
+        tot = pg[m, b]
+        at = pl.ds(b * CW, CW)
+        if b == 0:
+            o_loads[2 * m].wait()
+            o_loads[2 * m + 1].wait()
+        sb_in[m, b].arrived()
         for i in range(len(OFFSETS)):
-            tot = tot + recv_b[m, i].astype(F32)
-        f = beta_first * old[m, 0] + (1.0 - beta_first) * tot
-        s = beta_second * old[m, 1] + (1.0 - beta_second) * tot * tot
-        dirg[m, chip, c] = (f / (jnp.sqrt(s) + tiny_eps)).astype(BF16)
+            tot = tot + recv_b[m, b, i].astype(F32)
+        f = beta_first * old[m, 0, :, at] + (1.0 - beta_first) * tot
+        s = beta_second * old[m, 1, :, at] + (1.0 - beta_second) * tot * tot
+        dirg[m, b, chip, c] = (f / (jnp.sqrt(s) + tiny_eps)).astype(BF16)
         for i in range(len(OFFSETS)):
-            dp[m, i].start()
-        new[m, 0] = f
-        new[m, 1] = s
-        for i, out in enumerate((fnew, snew)):
-            o = pltpu.make_async_copy(new.at[m, i], out, sem_new.at[m, i])
-            o.start()
-            f_outs.append(o)
-
-    def spread(m):
-        dp_in[m].arrived()
-        dm[m].start()
+            dp[m, b, i].start()
+        new[m, 0, :, at] = f
+        new[m, 1, :, at] = s
+
+    def spread(m, b):
+        dp_in[m, b].arrived()
+        dm[m, b].start()
+
+    def direction_of(m):
+        return jnp.concatenate([dirg[m, b].reshape(R, CW) for b in range(NH)], axis=1)
 
     def gram_of(m):
         f = factor_of(m)
@@ -323,8 +330,9 @@
             sq[m, q] = Send(ss.at[m], ssg.at[m, q], sq_in[m], along_x(q))
 
     def squares(m):
-        dm_in[m].arrived()
-        d = dirg[m].reshape(R, C)
+        for b in range(NH):
+            dm_in[m, b].arrived()
+        d = direction_of(m)
         e = jnp.dot(gram[m, 0], d, preferred_element_type=F32)
         e += jnp.dot(gram[m, 1], d, preferred_element_type=F32)
         p = jnp.sum((e * d.astype(F32)).reshape(R // 8, 8, C), axis=0)
@@ -334,9 +342,14 @@
         ss[m] = t
         for q in range(1, ntp):
             sq[m, q].start()
-        o = pltpu.make_async_copy(dirg.at[m], dir_out.at[m], sem_out.at[4 + m])
-        o.start()
-        f_outs.append(o)
+
+    def expand(m):
+        d = direction_of(m)
+        f = fg.at[m]
+        for b in range(NZ):
+            ex[m, pl.ds(b * NZ * NC, NZ * NC)] = jnp.dot(
+                f[b].reshape(D // NZ, R), d, preferred_element_type=F32
+            ).reshape(NZ * NC, NQ * QR, C)
 
     def total(m):
         t = ss[m]
@@ -344,9 +357,6 @@
         for q in range(1, ntp):
             t = t + ssg[m, q]
         sst[m] = t
-        o = pltpu.make_async_copy(sst.at[m], ss_out.at[m], sem_new.at[m, 2])
-        o.start()
-        f_outs.append(o)
 
     for x in f_loads:
         x.wait()
@@ -363,14 +373,16 @@
             x.start()
 
     hooks = {
-        (0, 1): lambda: (more_rows(), f_second(0)),
-        (0, 2): lambda: f_second(1),
-        (0, 3): lambda: w_second(range(WS)),
+        (0, 1): lambda: more_rows(),
+        (0, 2): lambda: f_second(0),
+        (0, 3): lambda: f_second(1),
+        (0, 6): lambda: f_mate(0, (0,)),
         (0, 7): lambda: f_across(0, (1, 3)),
-        (1, 0): lambda: (f_across(0, (2,)), f_mate(0, (0,))),
-        (1, 2): lambda: (f_across(1, (1, 3)), f_mate(1, (0,))),
-        (1, 4): lambda: (f_mate(0, (1, 3)), f_across(1, (2,))),
-        (1, 6): lambda: (f_mate(0, (2,)), w_third((0, 1))),
+        (1, 0): lambda: f_mate(1, (0,)),
+        (1, 1): lambda: f_across(1, (1, 3)),
+        (1, 2): lambda: (f_across(0, (2,)), w_second(range(WS))),
+        (1, 4): lambda: f_mate(0, (1, 3)),
+        (1, 5): lambda: (f_mate(0, (2,)), f_across(1, (2,))),
         (1, 7): lambda: f_mate(1, (1, 3)),
     }
     for m in range(2):
@@ -380,32 +392,37 @@
             if (m, n) in hooks:
                 hooks[m, n]()
     f_done(0)
-    project(0)
+    project(0, 0)
     f_mate(1, (2,))
-    w_third((2, 3))
-    scatter(0)
+    project(0, 1)
+    scatter(0, 0)
+    scatter(0, 1)
     f_done(1)
-    project(1)
+    project(1, 0)
+    project(1, 1)
+    scatter(1, 0)
+    scatter(1, 1)
+    w_have(range(WS))
+    w_mate((0, 1, 3))
     gram_of(0)
-    scatter(1)
-    moments(0, fnew_v, snew_v)
-    w_mate((0, 1, 3))
+    moments(0, 0)
+    moments(0, 1)
     gram_of(1)
-    spread(0)
-    moments(1, fnew_o, snew_o)
+    moments(1, 0)
+    moments(1, 1)
+    w_third(range(WS))
+    spread(0, 0)
+    spread(0, 1)
+    spread(1, 0)
+    spread(1, 1)
     squares(0)
+    squares(1)
     w_mate((2,))
-    spread(1)
-    squares(1)
-    wm_in.arrived()
-    for m in range(2):
-        o = pltpu.make_async_copy(wg.at[m], wg_out.at[m], sem_out.at[2 + m])
-        o.start()
-        f_outs.append(o)
+    expand(0)
+    expand(1)
     total(0)
     total(1)
-    for o in f_outs:
-        o.wait()
+    wm_in.arrived()
     for i, n in enumerate(out_bytes):
         all_of = tally.at[pl.ds(0, n)]
         pltpu.make_async_remote_copy(
@@ -416,61 +433,38 @@
 
 def finish_kernel(
     ntp,
-    fg_in, wg_in, dir_in, ss_in, fac_v, fac_o, w_v, w_o, fn_v, sn_v, fn_o, sn_o,
+    new, ss, wg, ex, w_v, w_o,
     step_v, upd_v, fnew_v, snew_v, copy_v, step_o, upd_o, fnew_o, snew_o, copy_o,
-    fg, wg, dirg, res, fac, w, mo, ss, st, up, sem_f, sem_w, sem_s, sem_o, sem_p,
+    res, w, st, up, sem_w, sem_s, sem_o,
 ):
-    _, D, R = fg.shape
-    C = wg.shape[2]
-    n_ch = sem_f.shape[1]
-    CH = D // n_ch
-    loads, outs = {}, []
-
-    def load(key, src, dst, sem):
-        loads[key] = pltpu.make_async_copy(src, dst, sem)
-        loads[key].start()
+    me = lax.axis_index("fs")
+    n, B, C = ex.shape[1:]
+    n_ch = sem_o.shape[1]
+    loads, outs = [], []
 
     def store(src, dst, sem):
         o = pltpu.make_async_copy(src, dst, sem)
         o.start()
         outs.append(o)
 
-    load("s", ss_in, ss, sem_s.at[0])
-    mo_out = ((fnew_v, snew_v), (fnew_o, snew_o))
     for m in range(2):
-        load(("d", m), dir_in.at[m], dirg.at[m], sem_s.at[1 + m])
+        loads.append(pltpu.make_async_copy((w_v, w_o)[m], w.at[m], sem_w.at[m]))
+        loads[m].start()
+        for i in range(2):
+            store(new.at[m, i], ((fnew_v, snew_v), (fnew_o, snew_o))[m][i], sem_s.at[m, i])
+    for m, (step, upd, copy) in enumerate(((step_v, upd_v, copy_v), (step_o, upd_o, copy_o))):
+        mean = jnp.sum(ss[m], keepdims=True) / (n * B * C * ntp)
+        scale = step_rate / jnp.sqrt(mean + scale_floor)
         for b in range(n_ch):
-            at = pl.ds(b * CH, CH)
-            load(("f", m, b), fg_in.at[m, at], fg.at[m, at], sem_f.at[m, b])
-            load(("w", m, b), wg_in.at[m, at], wg.at[m, at], sem_w.at[m, b])
-        load(("k", m), (fac_v, fac_o)[m], fac.at[m], sem_s.at[3 + m])
-        load(("g", m), (w_v, w_o)[m], w.at[m], sem_s.at[5 + m])
-        for i in range(2):
-            load(("m", m, i), ((fn_v, sn_v), (fn_o, sn_o))[m][i], mo.at[m, i], sem_p.at[m, i])
-    loads["s"].wait()
-    for m, (step, upd, copy) in enumerate(((step_v, upd_v, copy_v), (step_o, upd_o, copy_o))):
-        mean = jnp.sum(ss[m], keepdims=True) / (D * C * ntp)
-        scale = step_rate / jnp.sqrt(mean + scale_floor)
-        loads["d", m].wait()
-        d = dirg[m]
-        for b in range(n_ch):
-            at = pl.ds(b * CH, CH)
-            loads["f", m, b].wait()
-            loads["w", m, b].wait()
-            with jax.named_scope(f"fin_{m}_{b}"):
-                e = jnp.dot(fg[m, at], d, preferred_element_type=F32)
-                res[m, at] = (wg[m, at].astype(F32) - scale * e).astype(BF16)
+            at = pl.ds(b * (n // n_ch), n // n_ch)
+            res[m, at] = (wg[m, at].astype(F32) - scale * ex[m, at]).astype(BF16)
             store(res.at[m, at], copy.at[at], sem_o.at[m, b])
-        for i in range(2):
-            loads["m", m, i].wait()
-            store(mo.at[m, i], mo_out[m][i], sem_p.at[m, i])
-        loads["k", m].wait()
-        loads["g", m].wait()
-        s = scale * jnp.dot(fac[m], d, preferred_element_type=F32)
+        loads[m].wait()
+        s = scale * ex[m, me]
         st[m] = s
         up[m] = w[m] - s
-        store(st.at[m], step, sem_s.at[7 + m])
-        store(up.at[m], upd, sem_s.at[9 + m])
+        store(st.at[m], step, sem_s.at[m, 2])
+        store(up.at[m], upd, sem_s.at[m, 3])
     for o in outs:
         o.wait()
 
@@ -486,50 +480,46 @@
     B, R = value_factor.shape
     k = value_first.shape[0]
     np_ = NZ * NZ
+    vm = pl.BlockSpec(memory_space=pltpu.VMEM)
     hbm = pl.BlockSpec(memory_space=pl.ANY)
     mom = jax.ShapeDtypeStruct((k, C), F32)
     wide = jax.ShapeDtypeStruct((B, C), F32)
-    full = jax.ShapeDtypeStruct((D, C), BF16)
+    full = jax.ShapeDtypeStruct((n, B, C), BF16)
     dma = pltpu.SemaphoreType.DMA
     fg_shape = (2, NZ, NZ, NC, NQ, B // NQ, R)
-    wg_shape = (2, NZ, NZ, NC, WS, B // WS, C)
-    dir_shape = (2, np_, NC, k, C)
-    fn_v, sn_v, fn_o, sn_o, ss, fg, wg, dirg = pl.pallas_call(
+    new, ss, wg, ex = pl.pallas_call(
         functools.partial(gather_kernel, ntp),
-        out_shape=(mom,) * 4 + (
-            jax.ShapeDtypeStruct((2, 8, 128), F32),
-            jax.ShapeDtypeStruct(fg_shape, BF16),
-            jax.ShapeDtypeStruct(wg_shape, BF16),
-            jax.ShapeDtypeStruct(dir_shape, BF16),
+        out_shape=(
+            pltpu.VMEM((2, 2, k, C), F32),
+            pltpu.VMEM((2, 8, 128), F32),
+            pltpu.VMEM((2, NZ, NZ, NC, WS, B // WS, C), BF16),
+            pltpu.VMEM((2, n, B, C), F32),
         ),
         in_specs=[hbm] * 12,
-        out_specs=(hbm,) * 8,
+        out_specs=(vm,) * 4,
         scratch_shapes=[
             pltpu.VMEM((2, T, D), BF16),
             pltpu.VMEM((2, T, C), BF16),
             pltpu.VMEM((2, C, T), BF16),
             pltpu.VMEM((2, C, D), BF16),
             pltpu.VMEM(fg_shape, BF16),
-            pltpu.VMEM(wg_shape, BF16),
-            pltpu.VMEM((2, np_, NC, k, C), F32),
-            pltpu.VMEM((2, np_, k, C), BF16),
-            pltpu.VMEM((2, np_, k, C), BF16),
-            pltpu.VMEM((2, np_, k, C), BF16),
-            pltpu.VMEM((2, np_ - 1, k, C), BF16),
-            pltpu.VMEM((2, k, C), F32),
-            pltpu.VMEM(dir_shape, BF16),
+            pltpu.VMEM((2, NH, np_, NC, k, C // NH), F32),
+            pltpu.VMEM((2, NH, np_, k, C // NH), BF16),
+            pltpu.VMEM((2, NH, np_, k, C // NH), BF16),
+            pltpu.VMEM((2, NH, np_, k, C // NH), BF16),
+            pltpu.VMEM((2, NH, np_ - 1, k, C // NH), BF16),
+            pltpu.VMEM((2, NH, k, C // NH), F32),
+            pltpu.VMEM((2, NH, np_, NC, k, C // NH), BF16),
             pltpu.VMEM((2, 2, R, R), BF16),
             pltpu.VMEM((2, 8, 128), F32),
             pltpu.VMEM((2, ntp, 8, 128), F32),
-            pltpu.VMEM((2, 8, 128), F32),
             pltpu.VMEM((512, 16, 128), BF16),
             pltpu.VMEM((2, B, C), F32),
             pltpu.VMEM((2, 2, k, C), F32),
-            pltpu.VMEM((2, 2, k, C), F32),
-            dma((2, 4)), dma((2,)), dma((6,)), dma((8,)), dma((2, 3)), dma((N_SEMS,)), dma((N_SEMS,)),
+            dma((2, 4)), dma((2,)), dma((8,)), dma((N_SEMS,)), dma((N_SEMS,)),
         ],
         compiler_params=pltpu.CompilerParams(
-            collective_id=0, has_side_effects=True, vmem_limit_bytes=62_000_000
+            collective_id=0, has_side_effects=True, vmem_limit_bytes=50_000_000
         ),
         name="gather",
     )(
@@ -538,31 +528,22 @@
         value_first, output_first, value_second, output_second,
     )
     n_ch = 4
-    return pl.pallas_call(
+    outs = pl.pallas_call(
         functools.partial(finish_kernel, ntp),
         out_shape=(wide, wide, mom, mom, full) * 2,
-        in_specs=[hbm] * 12,
+        in_specs=[vm] * 4 + [hbm] * 2,
         out_specs=(hbm,) * 10,
         scratch_shapes=[
-            pltpu.VMEM((2, D, R), BF16),
-            pltpu.VMEM((2, D, C), BF16),
-            pltpu.VMEM((2, R, C), BF16),
-            pltpu.VMEM((2, D, C), BF16),
-            pltpu.VMEM((2, B, R), BF16),
-            pltpu.VMEM((2, B, C), F32),
-            pltpu.VMEM((2, 2, k, C), F32),
-            pltpu.VMEM((2, 8, 128), F32),
+            pltpu.VMEM((2, n, B, C), BF16),
             pltpu.VMEM((2, B, C), F32),
             pltpu.VMEM((2, B, C), F32),
-            dma((2, n_ch)), dma((2, n_ch)), dma((11,)), dma((2, n_ch)), dma((2, 2)),
+            pltpu.VMEM((2, B, C), F32),
+            dma((2,)), dma((2, 4)), dma((2, n_ch)),
         ],
-        compiler_params=pltpu.CompilerParams(vmem_limit_bytes=62_000_000),
+        compiler_params=pltpu.CompilerParams(vmem_limit_bytes=20_000_000),
         name="finish",
-    )(
-        fg.reshape(2, D, R), wg.reshape(2, D, C), dirg.reshape(2, R, C), ss,
-        value_factor, output_factor, value_weight, output_weight,
-        fn_v, sn_v, fn_o, sn_o,
-    )
+    )(new, ss, wg.reshape(2, n, B, C), ex, value_weight, output_weight)
+    return tuple(o.reshape(D, C) if o.ndim == 3 else o for o in outs)
 
 
 def solution(mesh):

time: 61.6 us -> 52.7 us (0.86)
  Pallas kernels: 60.7 us -> 51.7 us
    pallas_call x1, Pallas kernels: 53.8 us -> 48 us  [local(): pl.pallas_call(functools.partial(gather_kernel, ntp), out_shape=(pltpu.VM...]
    pallas_call x1, Pallas kernels: 6.88 us -> 3.75 us  [local(): pl.pallas_call(functools.partial(finish_kernel, ntp), out_shape=(wide, wi...]
where the time goes in v3:
time: 52.7 us; the launch traced here: 52.6 us
  Pallas kernels  51.7 us (98%)
  between operations  0.85 us (2%)
    pallas_call x1, Pallas kernels, local(): pl.pallas_call(functools.partial(gather_kernel, ntp), out_shape=(pltpu.VM...  48 us
    pallas_call x1, Pallas kernels, local(): pl.pallas_call(functools.partial(finish_kernel, ntp), out_shape=(wide, wi...  3.75 us

profile of v3, /device:TPU:1, one launch (start us, length us, event | category | flops | bytes accessed | tf_op | source)
XLA Modules:
  0.0 52.6 jit_solution(15141462660576560814)
XLA Ops:
  0.6 0.0 copy-start
  0.7 0.0 copy-start.1
  0.7 48.0 %gather.1 = (f32[2,2,16,512]{3,2,1,0:T(8,128)S(1)}, f32[2,8,128]{2,1,0:T(8,128)S(1)}, bf16[2,4,4,2,4,16,512]{6,5,4,3,2,1,0:T(8,128)(2,1)S(1)}, f32[2,32,64,512]{3,2,1,0:T(8,128)S(1)}) custom-call(bf16[2048,2048]{1,0:T(8,128)(2,1)} %rows_v.1, bf16[2048,512]{1,0:T(8,128)(2,1)} %cols_v.1, bf16[2048,2048]{1,0:T(8,128)(2,1)} %rows_o.1, bf16[2048,512]{1,0:T(8,128)(2,1)} %cols_o.1, ...), custom_call_target="tpu_custom_call" | custom-call | tf_op jit(solution)/shard_map/gather/pallas_call | solution.py:490
  48.6 0.0 copy-done
  48.7 0.0 copy-done.1
  48.7 3.8 %finish.1 = (f32[64,512]{1,0:T(8,128)}, f32[64,512]{1,0:T(8,128)}, f32[16,512]{1,0:T(8,128)}, f32[16,512]{1,0:T(8,128)}, bf16[32,64,512]{2,1,0:T(8,128)(2,1)}, /...) custom-call(f32[2,2,16,512]{3,2,1,0:T(8,128)S(1)} %get-tuple-element, ...), custom_call_target="tpu_custom_call" | custom-call | tf_op jit(solution)/shard_map/finish/pallas_call | solution.py:531
Async XLA Ops:
  0.6 48.0 %copy-start = (f32[64,512]{1,0:T(8,128)S(1)}, f32[64,512]{1,0:T(8,128)}, u32[]{:S(2)}) copy-start(f32[64,512]{1,0:T(8,128)} %w_v.3) | copy-start | bytes 393220
  0.7 48.0 %copy-start.1 = (f32[64,512]{1,0:T(8,128)S(1)}, f32[64,512]{1,0:T(8,128)}, u32[]{:S(2)}) copy-start(f32[64,512]{1,0:T(8,128)} %w_o.3) | copy-start | bytes 393220

commit v4 on v3

--- a/solution.py
+++ b/solution.py
@@ -22,7 +22,7 @@
 NQ = 4
 WS = 4
 NH = 2
-N_SEMS = 64
+N_SEND, N_RECV = 6, 36
 OFFSETS = sorted(
     [(a, b) for a in range(NZ) for b in range(NZ) if a or b],
     key=lambda o: -(min(o[0], NZ - o[0]) + min(o[1], NZ - o[1])),
@@ -34,7 +34,7 @@
     rows_v, cols_v, rows_o, cols_o,
     fac_v, fac_o, w_v, w_o, first_v, first_o, second_v, second_o,
     new, sst, wg, ex,
-    rows, cols, cols_t, grad, fg, pf, send_a, recv_a, send_b, recv_b, pg,
+    rows, cols, cols_t, grad, fg, pf, send_a, recv_a, send_b, recv_b, mdir,
     dirg, gram, ss, ssg, tally, wide, old,
     sem_rows, sem_cols, sem_in, ssem, rsem,
 ):
@@ -58,10 +58,13 @@
     def plane(zz, yy):
         return ((zz * NZ + yy) * NC + c, tp)
 
+    def across(zz, yy):
+        return ((zz * NZ + yy) * NC + co, tp)
+
     mate = (me - c + co, tp)
 
-    def along_x(d):
-        return (me, lax.rem(tp + ntp + d, ntp))
+    def along_x(d, core=c):
+        return (me - c + core, lax.rem(tp + ntp + d, ntp))
 
     row_bytes = 2 * tally.shape[1] * tally.shape[2]
     n_recv = [0]
@@ -98,9 +101,13 @@
 
     barrier = pltpu.get_barrier_semaphore()
     for dz, dy in OFFSETS:
-        pl.semaphore_signal(barrier, inc=1, device_id=plane(up(z, dz), up(y, dy)), device_id_type=MESH)
+        pl.semaphore_signal(barrier, inc=1, device_id=across(up(z, dz), up(y, dy)), device_id_type=MESH)
+        if dz == 0 or dy == 0:
+            pl.semaphore_signal(barrier, inc=1, device_id=plane(up(z, dz), up(y, dy)), device_id_type=MESH)
     pl.semaphore_signal(barrier, inc=1, device_id=mate, device_id_type=MESH)
     for q in range(1, ntp):
+        pl.semaphore_signal(barrier, inc=1, device_id=along_x(q, co), device_id_type=MESH)
+    for q in (1, -1):
         pl.semaphore_signal(barrier, inc=1, device_id=along_x(q), device_id_type=MESH)
 
     half = D // 4
@@ -129,8 +136,8 @@
     def first_dev(s, d):
         return plane(up(z, d), y) if s == 0 else plane(z, up(y, d))
 
-    def second_dev(s, d):
-        return plane(z, up(y, d)) if s == 0 else plane(up(z, d), y)
+    def second_dev(s, d, to=plane):
+        return to(z, up(y, d)) if s == 0 else to(up(z, d), y)
 
     f1, f2, fx, fm, fxm = {}, {}, {}, {}, {}
     f1_in, f2_in, fx_in, fm_in = {}, {}, {}, {}
@@ -144,12 +151,13 @@
             k, kx = 2 * h + s, 2 * (1 - h) + s
             for d in (2, 1, 3):
                 f1[m, s, d] = Send(own(fg, m, s, 0, k), own(fg, m, s, 0, k), f1_in[m], first_dev(s, d))
-                f2[m, s, d] = Send(line(fg, m, s, 0, c, k), line(fg, m, s, 0, c, k), f2_in[m, d], second_dev(s, d))
+                f2[m, s, d] = Send(line(fg, m, s, 0, c, k), line(fg, m, s, 0, c, k), f2_in[m, d], second_dev(s, d, across))
             for g in range(NZ):
-                a, b = line(fg, m, s, g, c, k), line(fg, m, s, g, c, kx)
+                held = co if g else c
+                a, b = line(fg, m, s, g, held, k), line(fg, m, s, g, held, kx)
                 if g == 2:
                     o = line(fg, m, s, 0, c, kx)
-                    fx[m, s, g] = Send(o, o, fx_in[m, g], second_dev(s, 2))
+                    fx[m, s, g] = Send(o, o, fx_in[m, g], second_dev(s, 2, across))
                 else:
                     fx[m, s, g] = Send(a, a, fx_in[m, g], along_x(1 if s == 0 else -1))
                 fm[m, s, g] = Send(a, a, fm_in[m], mate)
@@ -195,14 +203,13 @@
         return wg.at[m, two, dn(y, g), c, j] if m == 0 else wg.at[m, dn(z, g), two, c, j]
 
     w1_in, w3_in, wm_in = Group(), Group(), Group()
-    w2_in = {}
+    w2_in = Group()
     for j in range(WS):
-        w2_in[j] = Group()
         for m in range(2):
             for d in (2, 1, 3):
                 w1[m, j, d] = Send(own(wg, m, m, 0, j), own(wg, m, m, 0, j), w1_in, first_dev(m, d))
             for d in (1, 3):
-                w2[m, j, d] = Send(line(wg, m, m, 0, c, j), line(wg, m, m, 0, c, j), w2_in[j], second_dev(m, d))
+                w2[m, j, d] = Send(line(wg, m, m, 0, c, j), line(wg, m, m, 0, c, j), w2_in, second_dev(m, d))
                 b = d // 2
                 w3[m, j, d] = Send(part(m, j, d, b), part(m, j, d, b), w3_in, second_dev(m, d))
     for m in range(2):
@@ -221,20 +228,18 @@
                 for m in range(2):
                     w1[m, j, d].start()
 
-    def w_second(js):
-        if js[0] == 0:
-            w1_in.arrived()
-        for j in js:
+    def w_second():
+        w1_in.arrived()
+        for j in range(WS):
             for d in (1, 3):
                 for m in range(2):
                     w2[m, j, d].start()
 
-    def w_have(js):
-        for j in js:
-            w2_in[j].arrived()
-
-    def w_third(js):
-        for j in js:
+    def w_have():
+        w2_in.arrived()
+
+    def w_third():
+        for j in range(WS):
             for d in (1, 3):
                 for m in range(2):
                     w3[m, j, d].start()
@@ -245,6 +250,9 @@
         for g in gs:
             for m in range(2):
                 wm[m, g].start()
+
+    def w_done():
+        wm_in.arrived()
 
     def turn_cols(m):
         col_loads[m].wait()
@@ -270,40 +278,42 @@
             p = m, b
             sa_in[p], sb_in[p], dp_in[p], dm_in[p] = Group(), Group(), Group(), Group()
             sa[p] = Send(send_a.at[m, b], recv_a.at[m, b], sa_in[p], mate)
-            mine = dirg.at[m, b, chip, c]
+            mine = mdir.at[m, b]
             for i, (dz, dy) in enumerate(OFFSETS):
                 to = up(z, dz) * NZ + up(y, dy)
-                dev = plane(up(z, dz), up(y, dy))
+                dev = across(up(z, dz), up(y, dy))
                 sb[m, b, i] = Send(send_b.at[m, b, to], recv_b.at[m, b, i], sb_in[p], dev)
-                dp[m, b, i] = Send(mine, mine, dp_in[p], dev)
-            dm[p] = Send(dirg.at[m, b, :, c], dirg.at[m, b, :, c], dm_in[p], mate)
+                dp[m, b, i] = Send(mine, dirg.at[m, b, chip, c], dp_in[p], dev)
+            i = len(OFFSETS)
+            sb[m, b, i] = Send(send_b.at[m, b, chip], recv_b.at[m, b, i], sb_in[p], mate)
+            dp[m, b, i] = Send(mine, dirg.at[m, b, chip, c], dp_in[p], mate)
+            dm[p] = Send(dirg.at[m, b, :, co], dirg.at[m, b, :, co], dm_in[p], mate)
 
     def project(m, b):
         pt = jnp.dot(grad[m, pl.ds(b * CW, CW)], factor_of(m), preferred_element_type=F32)
         pf[m, b] = pt.T.reshape(NZ * NZ, NC, QR, CW)
-        send_a[m, b] = pf[m, b, :, co].astype(BF16)
+        send_a[m, b] = pf[m, b, :, c].astype(BF16)
         sa[m, b].start()
 
     def scatter(m, b):
         sa_in[m, b].arrived()
-        send_b[m, b] = (pf[m, b, :, c] + recv_a[m, b].astype(F32)).astype(BF16)
-        for i in range(len(OFFSETS)):
+        send_b[m, b] = (pf[m, b, :, co] + recv_a[m, b].astype(F32)).astype(BF16)
+        for i in range(len(OFFSETS) + 1):
             sb[m, b, i].start()
-        pg[m, b] = pf[m, b, chip, c] + recv_a[m, b, chip].astype(F32)
 
     def moments(m, b):
-        tot = pg[m, b]
         at = pl.ds(b * CW, CW)
         if b == 0:
             o_loads[2 * m].wait()
             o_loads[2 * m + 1].wait()
         sb_in[m, b].arrived()
-        for i in range(len(OFFSETS)):
+        tot = recv_b[m, b, 0].astype(F32)
+        for i in range(1, len(OFFSETS) + 1):
             tot = tot + recv_b[m, b, i].astype(F32)
         f = beta_first * old[m, 0, :, at] + (1.0 - beta_first) * tot
         s = beta_second * old[m, 1, :, at] + (1.0 - beta_second) * tot * tot
-        dirg[m, b, chip, c] = (f / (jnp.sqrt(s) + tiny_eps)).astype(BF16)
-        for i in range(len(OFFSETS)):
+        mdir[m, b] = (f / (jnp.sqrt(s) + tiny_eps)).astype(BF16)
+        for i in range(len(OFFSETS) + 1):
             dp[m, b, i].start()
         new[m, 0, :, at] = f
         new[m, 1, :, at] = s
@@ -327,7 +337,7 @@
     for m in range(2):
         sq_in[m] = Group()
         for q in range(1, ntp):
-            sq[m, q] = Send(ss.at[m], ssg.at[m, q], sq_in[m], along_x(q))
+            sq[m, q] = Send(ss.at[m], ssg.at[m, q], sq_in[m], along_x(q, co))
 
     def squares(m):
         for b in range(NH):
@@ -343,10 +353,10 @@
         for q in range(1, ntp):
             sq[m, q].start()
 
-    def expand(m):
+    def expand(m, bs):
         d = direction_of(m)
         f = fg.at[m]
-        for b in range(NZ):
+        for b in bs:
             ex[m, pl.ds(b * NZ * NC, NZ * NC)] = jnp.dot(
                 f[b].reshape(D // NZ, R), d, preferred_element_type=F32
             ).reshape(NZ * NC, NQ * QR, C)
@@ -358,9 +368,11 @@
             t = t + ssg[m, q]
         sst[m] = t
 
+    assert (len(out_bytes), n_recv[0]) == (N_SEND, N_RECV)
+
     for x in f_loads:
         x.wait()
-    pl.semaphore_wait(barrier, len(OFFSETS) + 1 + ntp - 1)
+    pl.semaphore_wait(barrier, len(OFFSETS) + 2 * (NZ - 1) + 1 + (ntp - 1) + 2)
     f_first(0)
     f_first(1)
     w_own()
@@ -380,7 +392,7 @@
         (0, 7): lambda: f_across(0, (1, 3)),
         (1, 0): lambda: f_mate(1, (0,)),
         (1, 1): lambda: f_across(1, (1, 3)),
-        (1, 2): lambda: (f_across(0, (2,)), w_second(range(WS))),
+        (1, 2): lambda: (f_across(0, (2,)), w_second()),
         (1, 4): lambda: f_mate(0, (1, 3)),
         (1, 5): lambda: (f_mate(0, (2,)), f_across(1, (2,))),
         (1, 7): lambda: f_mate(1, (1, 3)),
@@ -402,7 +414,7 @@
     project(1, 1)
     scatter(1, 0)
     scatter(1, 1)
-    w_have(range(WS))
+    w_have()
     w_mate((0, 1, 3))
     gram_of(0)
     moments(0, 0)
@@ -410,19 +422,20 @@
     gram_of(1)
     moments(1, 0)
     moments(1, 1)
-    w_third(range(WS))
+    w_third()
     spread(0, 0)
     spread(0, 1)
     spread(1, 0)
     spread(1, 1)
     squares(0)
+    expand(0, (0, 1))
     squares(1)
     w_mate((2,))
-    expand(0)
-    expand(1)
+    expand(0, (2, 3))
+    expand(1, range(NZ))
     total(0)
     total(1)
-    wm_in.arrived()
+    w_done()
     for i, n in enumerate(out_bytes):
         all_of = tally.at[pl.ds(0, n)]
         pltpu.make_async_remote_copy(
@@ -452,13 +465,20 @@
         loads[m].start()
         for i in range(2):
             store(new.at[m, i], ((fnew_v, snew_v), (fnew_o, snew_o))[m][i], sem_s.at[m, i])
+    per = n // n_ch
     for m, (step, upd, copy) in enumerate(((step_v, upd_v, copy_v), (step_o, upd_o, copy_o))):
         mean = jnp.sum(ss[m], keepdims=True) / (n * B * C * ntp)
         scale = step_rate / jnp.sqrt(mean + scale_floor)
+
+        @pl.loop(0, n_ch)
+        def _(b):
+            at = pl.ds(pl.multiple_of(b * per, per), per)
+            res[m, at] = (wg[m, at].astype(F32) - scale * ex[m, at]).astype(BF16)
+            pltpu.make_async_copy(res.at[m, at], copy.at[at], sem_o.at[m, b]).start()
+
         for b in range(n_ch):
-            at = pl.ds(b * (n // n_ch), n // n_ch)
-            res[m, at] = (wg[m, at].astype(F32) - scale * ex[m, at]).astype(BF16)
-            store(res.at[m, at], copy.at[at], sem_o.at[m, b])
+            at = pl.ds(b * per, per)
+            outs.append(pltpu.make_async_copy(res.at[m, at], copy.at[at], sem_o.at[m, b]))
         loads[m].wait()
         s = scale * ex[m, me]
         st[m] = s
@@ -507,8 +527,8 @@
             pltpu.VMEM((2, NH, np_, k, C // NH), BF16),
             pltpu.VMEM((2, NH, np_, k, C // NH), BF16),
             pltpu.VMEM((2, NH, np_, k, C // NH), BF16),
-            pltpu.VMEM((2, NH, np_ - 1, k, C // NH), BF16),
-            pltpu.VMEM((2, NH, k, C // NH), F32),
+            pltpu.VMEM((2, NH, np_, k, C // NH), BF16),
+            pltpu.VMEM((2, NH, k, C // NH), BF16),
             pltpu.VMEM((2, NH, np_, NC, k, C // NH), BF16),
             pltpu.VMEM((2, 2, R, R), BF16),
             pltpu.VMEM((2, 8, 128), F32),
@@ -516,7 +536,7 @@
             pltpu.VMEM((512, 16, 128), BF16),
             pltpu.VMEM((2, B, C), F32),
             pltpu.VMEM((2, 2, k, C), F32),
-            dma((2, 4)), dma((2,)), dma((8,)), dma((N_SEMS,)), dma((N_SEMS,)),
+            dma((2, 4)), dma((2,)), dma((8,)), dma((N_SEND,)), dma((N_RECV,)),
         ],
         compiler_params=pltpu.CompilerParams(
             collective_id=0, has_side_effects=True, vmem_limit_bytes=50_000_000

time: 52.7 us -> 51.4 us (0.975)
  Pallas kernels: 51.7 us -> 50.4 us
    pallas_call x1, Pallas kernels: 3.75 us -> 2.92 us  [local(): pl.pallas_call(functools.partial(finish_kernel, ntp), out_shape=(wide, wi...]
where the time goes in v4:
time: 51.4 us; the launch traced here: 51.3 us
  Pallas kernels  50.4 us (98%)
  between operations  0.85 us (2%)
    pallas_call x1, Pallas kernels, local(): pl.pallas_call(functools.partial(gather_kernel, ntp), out_shape=(pltpu.VM...  47.5 us
    pallas_call x1, Pallas kernels, local(): pl.pallas_call(functools.partial(finish_kernel, ntp), out_shape=(wide, wi...  2.92 us

profile of v4, /device:TPU:1, one launch (start us, length us, event | category | flops | bytes accessed | tf_op | source)
XLA Modules:
  0.0 51.3 jit_solution(2690714508082456407)
XLA Ops:
  0.6 0.0 copy-start
  0.7 0.0 copy-start.1
  0.7 47.5 %gather.1 = (f32[2,2,16,512]{3,2,1,0:T(8,128)S(1)}, f32[2,8,128]{2,1,0:T(8,128)S(1)}, bf16[2,4,4,2,4,16,512]{6,5,4,3,2,1,0:T(8,128)(2,1)S(1)}, f32[2,32,64,512]{3,2,1,0:T(8,128)S(1)}) custom-call(bf16[2048,2048]{1,0:T(8,128)(2,1)} %rows_v.1, bf16[2048,512]{1,0:T(8,128)(2,1)} %cols_v.1, bf16[2048,2048]{1,0:T(8,128)(2,1)} %rows_o.1, bf16[2048,512]{1,0:T(8,128)(2,1)} %cols_o.1, ...), custom_call_target="tpu_custom_call" | custom-call | tf_op jit(solution)/shard_map/gather/pallas_call | solution.py:510
  48.2 0.0 copy-done
  48.2 0.0 copy-done.1
  48.2 2.9 %finish.1 = (f32[64,512]{1,0:T(8,128)}, f32[64,512]{1,0:T(8,128)}, f32[16,512]{1,0:T(8,128)}, f32[16,512]{1,0:T(8,128)}, bf16[32,64,512]{2,1,0:T(8,128)(2,1)}, /...) custom-call(f32[2,2,16,512]{3,2,1,0:T(8,128)S(1)} %get-tuple-element, ...), custom_call_target="tpu_custom_call" | custom-call | tf_op jit(solution)/shard_map/finish/pallas_call | solution.py:551
Async XLA Ops:
  0.6 47.5 %copy-start = (f32[64,512]{1,0:T(8,128)S(1)}, f32[64,512]{1,0:T(8,128)}, u32[]{:S(2)}) copy-start(f32[64,512]{1,0:T(8,128)} %w_v.3) | copy-start | bytes 393220
  0.7 47.5 %copy-start.1 = (f32[64,512]{1,0:T(8,128)S(1)}, f32[64,512]{1,0:T(8,128)}, u32[]{:S(2)}) copy-start(f32[64,512]{1,0:T(8,128)} %w_o.3) | copy-start | bytes 393220

commit v5 on v4

--- a/solution.py
+++ b/solution.py
@@ -388,14 +388,12 @@
         (0, 1): lambda: more_rows(),
         (0, 2): lambda: f_second(0),
         (0, 3): lambda: f_second(1),
-        (0, 6): lambda: f_mate(0, (0,)),
-        (0, 7): lambda: f_across(0, (1, 3)),
+        (0, 7): lambda: (f_mate(0, (0,)), f_across(0, (1, 3))),
         (1, 0): lambda: f_mate(1, (0,)),
         (1, 1): lambda: f_across(1, (1, 3)),
         (1, 2): lambda: (f_across(0, (2,)), w_second()),
-        (1, 4): lambda: f_mate(0, (1, 3)),
-        (1, 5): lambda: (f_mate(0, (2,)), f_across(1, (2,))),
-        (1, 7): lambda: f_mate(1, (1, 3)),
+        (1, 4): lambda: f_across(1, (2,)),
+        (1, 5): lambda: (f_mate(0, (1, 3)), f_mate(0, (2,))),
     }
     for m in range(2):
         turn_cols(m)
@@ -405,24 +403,25 @@
                 hooks[m, n]()
     f_done(0)
     project(0, 0)
+    f_mate(1, (1, 3))
     f_mate(1, (2,))
     project(0, 1)
     scatter(0, 0)
-    scatter(0, 1)
     f_done(1)
     project(1, 0)
+    scatter(0, 1)
     project(1, 1)
     scatter(1, 0)
     scatter(1, 1)
-    w_have()
-    w_mate((0, 1, 3))
     gram_of(0)
     moments(0, 0)
     moments(0, 1)
     gram_of(1)
     moments(1, 0)
     moments(1, 1)
+    w_have()
     w_third()
+    w_mate((0, 1, 3))
     spread(0, 0)
     spread(0, 1)
     spread(1, 0)

time: 51.4 us -> 50.8 us (0.988)
    pallas_call x1, Pallas kernels: 47.5 us -> 47 us  [local(): pl.pallas_call(functools.partial(gather_kernel, ntp), out_shape=(pltpu.VM...]
where the time goes in v5:
time: 50.8 us; the launch traced here: 50.7 us
  Pallas kernels  49.9 us (98%)
  between operations  0.85 us (2%)
    pallas_call x1, Pallas kernels, local(): pl.pallas_call(functools.partial(gather_kernel, ntp), out_shape=(pltpu.VM...  47 us
    pallas_call x1, Pallas kernels, local(): pl.pallas_call(functools.partial(finish_kernel, ntp), out_shape=(wide, wi...  2.92 us

profile of v5, /device:TPU:1, one launch (start us, length us, event | category | flops | bytes accessed | tf_op | source)
XLA Modules:
  0.0 50.7 jit_solution(18293525396511650193)
XLA Ops:
  0.6 0.0 copy-start
  0.7 0.0 copy-start.1
  0.7 47.0 %gather.1 = (f32[2,2,16,512]{3,2,1,0:T(8,128)S(1)}, f32[2,8,128]{2,1,0:T(8,128)S(1)}, bf16[2,4,4,2,4,16,512]{6,5,4,3,2,1,0:T(8,128)(2,1)S(1)}, f32[2,32,64,512]{3,2,1,0:T(8,128)S(1)}) custom-call(bf16[2048,2048]{1,0:T(8,128)(2,1)} %rows_v.1, bf16[2048,512]{1,0:T(8,128)(2,1)} %cols_v.1, bf16[2048,2048]{1,0:T(8,128)(2,1)} %rows_o.1, bf16[2048,512]{1,0:T(8,128)(2,1)} %cols_o.1, ...), custom_call_target="tpu_custom_call" | custom-call | tf_op jit(solution)/shard_map/gather/pallas_call | solution.py:509
  47.6 0.0 copy-done
  47.6 0.0 copy-done.1
  47.7 2.9 %finish.1 = (f32[64,512]{1,0:T(8,128)}, f32[64,512]{1,0:T(8,128)}, f32[16,512]{1,0:T(8,128)}, f32[16,512]{1,0:T(8,128)}, bf16[32,64,512]{2,1,0:T(8,128)(2,1)}, /...) custom-call(f32[2,2,16,512]{3,2,1,0:T(8,128)S(1)} %get-tuple-element, ...), custom_call_target="tpu_custom_call" | custom-call | tf_op jit(solution)/shard_map/finish/pallas_call | solution.py:550
Async XLA Ops:
  0.6 47.0 %copy-start = (f32[64,512]{1,0:T(8,128)S(1)}, f32[64,512]{1,0:T(8,128)}, u32[]{:S(2)}) copy-start(f32[64,512]{1,0:T(8,128)} %w_v.3) | copy-start | bytes 393220
  0.7 47.0 %copy-start.1 = (f32[64,512]{1,0:T(8,128)S(1)}, f32[64,512]{1,0:T(8,128)}, u32[]{:S(2)}) copy-start(f32[64,512]{1,0:T(8,128)} %w_o.3) | copy-start | bytes 393220

commit v6 on v5

--- a/solution.py
+++ b/solution.py
@@ -425,12 +425,12 @@
     spread(0, 0)
     spread(0, 1)
     spread(1, 0)
+    squares(0)
     spread(1, 1)
-    squares(0)
-    expand(0, (0, 1))
+    expand(0, (0, 1, 2))
     squares(1)
     w_mate((2,))
-    expand(0, (2, 3))
+    expand(0, (3,))
     expand(1, range(NZ))
     total(0)
     total(1)

time: 50.8 us -> 50.5 us (level)
  no operation moved by 1% of the time
where the time goes in v6:
time: 50.5 us; the launch traced here: 50.4 us
  Pallas kernels  49.5 us (98%)
  between operations  0.85 us (2%)
    pallas_call x1, Pallas kernels, local(): pl.pallas_call(functools.partial(gather_kernel, ntp), out_shape=(pltpu.VM...  46.6 us
    pallas_call x1, Pallas kernels, local(): pl.pallas_call(functools.partial(finish_kernel, ntp), out_shape=(wide, wi...  2.92 us

profile of v6, /device:TPU:1, one launch (start us, length us, event | category | flops | bytes accessed | tf_op | source)
XLA Modules:
  0.0 50.4 jit_solution(13464581013181899132)
XLA Ops:
  0.6 0.0 copy-start
  0.7 0.0 copy-start.1
  0.7 46.6 %gather.1 = (f32[2,2,16,512]{3,2,1,0:T(8,128)S(1)}, f32[2,8,128]{2,1,0:T(8,128)S(1)}, bf16[2,4,4,2,4,16,512]{6,5,4,3,2,1,0:T(8,128)(2,1)S(1)}, f32[2,32,64,512]{3,2,1,0:T(8,128)S(1)}) custom-call(bf16[2048,2048]{1,0:T(8,128)(2,1)} %rows_v.1, bf16[2048,512]{1,0:T(8,128)(2,1)} %cols_v.1, bf16[2048,2048]{1,0:T(8,128)(2,1)} %rows_o.1, bf16[2048,512]{1,0:T(8,128)(2,1)} %cols_o.1, ...), custom_call_target="tpu_custom_call" | custom-call | tf_op jit(solution)/shard_map/gather/pallas_call | solution.py:509
  47.3 0.0 copy-done
  47.3 0.0 copy-done.1
  47.3 2.9 %finish.1 = (f32[64,512]{1,0:T(8,128)}, f32[64,512]{1,0:T(8,128)}, f32[16,512]{1,0:T(8,128)}, f32[16,512]{1,0:T(8,128)}, bf16[32,64,512]{2,1,0:T(8,128)(2,1)}, /...) custom-call(f32[2,2,16,512]{3,2,1,0:T(8,128)S(1)} %get-tuple-element, ...), custom_call_target="tpu_custom_call" | custom-call | tf_op jit(solution)/shard_map/finish/pallas_call | solution.py:550
Async XLA Ops:
  0.6 46.6 %copy-start = (f32[64,512]{1,0:T(8,128)S(1)}, f32[64,512]{1,0:T(8,128)}, u32[]{:S(2)}) copy-start(f32[64,512]{1,0:T(8,128)} %w_v.3) | copy-start | bytes 393220
  0.7 46.6 %copy-start.1 = (f32[64,512]{1,0:T(8,128)S(1)}, f32[64,512]{1,0:T(8,128)}, u32[]{:S(2)}) copy-start(f32[64,512]{1,0:T(8,128)} %w_o.3) | copy-start | bytes 393220
